TPU v7x, 128 devices: a whole 4x4x4 slice. The times are simulated.
128 devices in a mesh: sp: 16 (over z, x), tp: 8 (over y, core).
Axes of the slice: x: 4, y: 4, z: 4, core: 2. Of those that a mesh axis runs over, the one named last changes fastest.
Arguments:
- out_gate: bfloat16 [16384, 1536], P('sp', 'tp'), may hold values from -6 to 6
- in_gate: bfloat16 [16384, 1536], P('sp', 'tp'), may hold values from -6 to 6
- conv_values: bfloat16 [16384, 1536], P('sp', 'tp'), may hold values from -6 to 6
- conv_taps: float32 [3, 1536], P(None, 'tp'), may hold values from -3 to 3
- mix_gain: float32 [1536], replicated, may hold values from 0.1 to 1.9
- out_proj: bfloat16 [1536, 2048], replicated, may hold values from -0.15625 to 0.15625
- residual: bfloat16 [16384, 2048], P(('sp', 'tp')), may hold values from -6 to 6
- ffn_gain: float32 [2048], replicated, may hold values from 0.1 to 1.9
- routes: int32 [16384, 6], P(('sp', 'tp')), may hold values from 0 to 127, all different within a row; in each aligned block of 128 rows (0 to 127, 128 to 255, ...) at most 8 rows name the same one
- route_weights: float32 [16384, 6], P(('sp', 'tp')), may hold values from 0.05 to 1
- shared_gate: bfloat16 [2048, 512], replicated, may hold values from -0.125 to 0.125
- shared_up: bfloat16 [2048, 512], replicated, may hold values from -0.125 to 0.125
- shared_down: bfloat16 [512, 2048], replicated, may hold values from -0.25 to 0.25
- expert_gate: bfloat16 [128, 2048, 512], P(('sp', 'tp')), may hold values from -0.125 to 0.125
- expert_up: bfloat16 [128, 2048, 512], P(('sp', 'tp')), may hold values from -0.125 to 0.125
- expert_down: bfloat16 [128, 512, 2048], P(('sp', 'tp')), may hold values from -0.25 to 0.25
Outputs:
- layer_out: bfloat16 [16384, 2048], P(('sp', 'tp'))
Inputs may be any that keep to these rules, and one draw needn't show every extreme that they name: `routes`: each row names 6 different experts. Within the rows of one device (aligned blocks of 128 rows) no expert is named more than 8 times, a bound that some block reaches.
All inputs are finite; a program needn't handle non-finite values.
Results may differ from a plain program's by a relative error of at most 0.0065.
Values may be sent and summed in bfloat16 or wider, within the bound.
A program may use at most 128 MiB of HBM per device.

v0:
```python
import jax
import jax.numpy as jnp
from jax import lax
from jax.sharding import PartitionSpec as P


def from_behind(block, axis, distance):
    devices = range(lax.axis_size(axis))
    route = [(i - distance, i) for i in devices if i - distance in devices]
    return lax.ppermute(block, axis, route)


def project_norm(conv_out, mix_gain, out_proj):
    values = conv_out.astype(jnp.float32)
    inverse = lax.rsqrt(jnp.mean(values * values, axis=-1) + 1e-06)
    scaled = (values * mix_gain).astype(jnp.bfloat16)
    return jnp.dot(scaled, out_proj, preferred_element_type=jnp.float32) * inverse[:, None]


def swiglu_hidden(row_block, weight_gate, weight_up):
    gate_part = jnp.dot(row_block, weight_gate, preferred_element_type=jnp.float32)
    up_part = jnp.dot(row_block, weight_up, preferred_element_type=jnp.float32)
    return (jax.nn.silu(gate_part) * up_part).astype(jnp.bfloat16)


def body(
    out_gate,
    in_gate,
    conv_values,
    conv_taps,
    mix_gain,
    out_proj,
    residual,
    ffn_gain,
    routes,
    route_weights,
    shared_gate,
    shared_up,
    shared_down,
    expert_gate,
    expert_up,
    expert_down,
):
    mixed_in = in_gate.astype(jnp.float32) * conv_values.astype(jnp.float32)
    taps_count = conv_taps.shape[0]
    length = mixed_in.shape[0]
    earlier = from_behind(mixed_in[length - (taps_count - 1) :], "sp", 1)
    extended = jnp.concatenate([earlier, mixed_in], axis=0)
    filtered = conv_taps[0] * extended[0:length]
    for offset in range(1, taps_count):
        filtered = filtered + conv_taps[offset] * extended[offset : offset + length]
    conv_out = (out_gate.astype(jnp.float32) * filtered).astype(jnp.bfloat16)
    row_count = length // lax.axis_size("tp")
    token_rows = lax.all_to_all(conv_out, "tp", split_axis=0, concat_axis=1, tiled=True)
    mix_result = project_norm(token_rows, mix_gain, out_proj)
    stream = residual.astype(jnp.float32) + mix_result
    norm_inverse = lax.rsqrt(jnp.mean(stream * stream, axis=-1, keepdims=True) + 1e-06)
    normed = (stream * norm_inverse * ffn_gain).astype(jnp.bfloat16)
    shared_result = jnp.dot(
        swiglu_hidden(normed, shared_gate, shared_up),
        shared_down,
        preferred_element_type=jnp.float32,
    )
    model_width = normed.shape[1]
    sp_count = lax.axis_size("sp")
    tp_count = lax.axis_size("tp")
    experts_total = sp_count * tp_count
    top_count = routes.shape[1]
    capacity = max(2, 4 * row_count * top_count // (3 * experts_total))
    flat_ids = routes.reshape(-1)
    onehot = (flat_ids[:, None] == jnp.arange(experts_total, dtype=jnp.int32)[None, :]).astype(
        jnp.int32
    )
    before = jnp.cumsum(onehot, axis=0) - onehot
    slot_rank = jnp.sum(before * onehot, axis=1)
    slot_index = flat_ids * capacity + slot_rank
    source_rows = (
        jnp.full((experts_total * capacity,), row_count, jnp.int32)
        .at[slot_index]
        .set(jnp.arange(flat_ids.shape[0], dtype=jnp.int32) // top_count)
    )
    padded = jnp.concatenate([normed, jnp.zeros((1, model_width), jnp.bfloat16)], axis=0)
    outgoing = padded[source_rows].reshape(experts_total, capacity, model_width)
    arrived = lax.all_to_all(outgoing, ("sp", "tp"), split_axis=0, concat_axis=0, tiled=True)
    leading = arrived.shape[:-1]
    hidden = swiglu_hidden(arrived.reshape(-1, model_width), expert_gate[0], expert_up[0])
    result = jnp.dot(hidden, expert_down[0], preferred_element_type=jnp.float32).astype(
        jnp.bfloat16
    )
    returned_rows = lax.all_to_all(
        result.reshape(leading + (model_width,)),
        ("sp", "tp"),
        split_axis=0,
        concat_axis=0,
        tiled=True,
    )
    flat_returned = returned_rows.reshape(experts_total * capacity, model_width)
    picked = (
        flat_returned[slot_index].reshape(row_count, top_count, model_width).astype(jnp.float32)
    )
    gate_values = route_weights / jnp.sum(route_weights, axis=1, keepdims=True) * 2.5
    routed = jnp.sum(picked * gate_values[:, :, None], axis=1)
    return (stream + shared_result + routed).astype(jnp.bfloat16)


def solution(mesh):
    in_specs = (
        P("sp", "tp"),
        P("sp", "tp"),
        P("sp", "tp"),
        P(None, "tp"),
        P(),
        P(),
        P(("sp", "tp"), None),
        P(),
        P(("sp", "tp"), None),
        P(("sp", "tp"), None),
        P(),
        P(),
        P(),
        P(("sp", "tp"), None, None),
        P(("sp", "tp"), None, None),
        P(("sp", "tp"), None, None),
    )
    out_specs = P(("sp", "tp"), None)
    return jax.shard_map(body, mesh=mesh, in_specs=in_specs, out_specs=out_specs, check_vma=False)
```

profile of v0, /device:TPU:1, one launch (start us, length us, event | category | flops | bytes accessed | tf_op | source)
XLA Modules:
  0.0 201.5 jit_solution(9526734059948508831)
XLA Ops:
  0.0 0.0 copy-start
  0.0 1.4 convert_multiply_fusion
  1.4 0.7 slice.36
  2.1 4.5 %collective-permute-start = (f32[2,192]{0,1:T(8,128)}, f32[2,192]{0,1:T(8,128)}, u32[]{:S(2)}, u32[]{:S(2)}) collective-permute-start(f32[2,192]{0,1:T(8,128)} %slice.36), channel_id=1, source_target_pairs={{0,8},{8,16},{16,24},{24,32},{32,40},{40,48},{48,56},{56,64},{64,7... | collective-permute-start | bytes 4616 | tf_op jit(solution)/shard_map/ppermute | solution.py:10
  6.7 0.8 copy.33
  7.5 0.1 eq.29
  7.6 0.1 eq.25
  7.7 0.7 broadcast_multiply_fusion
  8.4 0.8 fusion.49
  9.2 0.1 copy.35
  9.3 0.2 fusion.28
  9.6 0.0 copy-start.6
  9.6 0.0 copy-start.8
  9.6 0.1 copy.36
  9.7 0.0 copy-start.5
  9.7 0.3 fusion.31
  10.0 0.0 collective-permute-done
  10.0 0.5 copy-done.6
  10.6 2.3 %copy_bitcast_fusion = bf16[8,128,192]{1,2,0:T(8,128)(2,1)} fusion(f32[1024,192]{0,1:T(8,128)S(1)} %convert_multiply_fusion, f32[192]{0:T(256)S(1)} %bitcast.61, f32[2,192]{0,1:T(8,128)} %collective-permute-done, f32[192]{0:T(256)S(1)} %bitcast.62, f32[192]{0:T(256)S(1)} %bitcast.60, bf16[1024,192]{0,1:T(8,128)(2,1)S(1)} %copy-done.6), kind=kLoop, calls=%fused_computation.40 | loop fusion | flops 1966080 | bytes 1576704 | tf_op jit(solution)/shard_map/all_to_all | solution.py:54
  12.9 5.4 %all-to-all-start = ((bf16[8,128,192]{1,2,0:T(8,128)(2,1)}), bf16[8,128,192]{1,2,0:T(8,128)(2,1)S(1)}, u32[]{:S(2)}, u32[]{:S(2)}) async-start(bf16[8,128,192]{1,2,0:T(8,128)(2,1)} %copy_bitcast_fusion), calls=%async_computation | async-start | bytes 786432 | tf_op jit(solution)/shard_map/all_to_all | solution.py:54
  18.3 0.1 copy.32
  18.4 0.1 mul.148
  18.6 3.4 %scatter_custom_fusion = s32[1024]{0:T(1024)S(1)} fusion(s32[768]{0:T(1024)S(1)} %fusion.44, s32[768]{0:T(1024)S(1)} %add_select_fusion, s32[]{:T(128)} %constant.13.clone.1), kind=kCustom, calls=%fused_computation.69 | custom fusion | bytes 4100 | tf_op jit(solution)/shard_map/scatter | solution.py:80
  22.0 4.0 %all-to-all-done = bf16[8,128,192]{1,2,0:T(8,128)(2,1)S(1)} async-done(((bf16[8,128,192]{1,2,0:T(8,128)(2,1)}), bf16[8,128,192]{1,2,0:T(8,128)(2,1)S(1)}, u32[]{:S(2)}, u32[]{:S(2)}) %all-to-all-start) | async-done | bytes 393248 | tf_op jit(solution)/shard_map/all_to_all | solution.py:54
  26.0 0.2 multiply_reduce_fusion.2
  26.2 0.0 copy-done.8
  26.2 0.3 fusion.27
  26.5 0.0 copy-done.5
  26.5 0.0 copy-start.9
  26.5 3.9 %multiply_reduce_fusion.1 = (f32[128]{0:T(128)S(1)}, f32[128,2048]{1,0:T(8,128)S(1)}) fusion(f32[128]{0:T(128)S(1)} %add_rsqrt_fusion.1, bf16[128,1536]{0,1:T(8,128)(2,1)S(1)} %fusion.27, bf16[1536,2048]{1,0:T(8,128)(2,1)} %param.21, bf16[128,2048]{1,0:T(8,128)(2,1)S(1)} %copy-done.5), kind=kOutput, calls=%fused_computation.22 | convolution fusion | flops 806616960 | bytes 8258560 | tf_op jit(solution)/shard_map/dot_general | solution.py:17
  30.4 0.0 copy-start.1
  30.5 1.0 copy-done.1
  31.4 0.0 copy-done.9
  31.4 0.2 multiply_convert_fusion.1
  31.6 0.0 copy-start.3
  31.6 6.0 %gather_fusion = bf16[1024,2048]{1,0:T(8,128)(2,1)} fusion(bf16[129,2048]{1,0:T(8,128)(2,1)S(1)} %concatenate.7, s32[1024]{0:T(1024)S(1)} %fusion.42), kind=kCustom, calls=%fused_computation | custom fusion | bytes 8392704 | tf_op jit(solution)/shard_map/gather | solution.py:83
  37.7 0.0 copy-start.10
  37.7 61.4 %all_to_all.23 = bf16[128,8,2048]{2,1,0:T(8,128)(2,1)S(1)} all-to-all(bf16[128,8,2048]{2,1,0:T(8,128)(2,1)} %bitcast.58), channel_id=1, replica_groups=mesh['sp'=16,'tp'=8] {'sp','tp'}, dimensions={0} | all-to-all | bytes 8388608 | tf_op jit(solution)/shard_map/all_to_all | solution.py:84
  99.0 0.0 copy-start.4
  99.0 2.0 copy-done.4
  101.0 0.0 copy-done.10
  101.0 3.7 %fusion.2 = f32[1024,512]{1,0:T(8,128)} fusion(bf16[128,8,2048]{2,1,0:T(8,128)(2,1)S(1)} %all_to_all.23, bf16[1,2048,512]{2,1,0:T(8,128)(2,1)S(1)} %copy-done.10), kind=kOutput, calls=%fused_computation.6 | convolution fusion | flops 2147483648 | bytes 8388608 | tf_op jit(solution)/shard_map/dot_general | solution.py:21
  104.7 0.0 copy-done
  104.7 10.0 %convert_bitcast_fusion = bf16[128,8,2048]{2,1,0:T(8,128)(2,1)} fusion(bf16[1,512,2048]{2,1,0:T(8,128)(2,1)S(1)} %copy-done, f32[1024,512]{1,0:T(8,128)} %fusion.2, bf16[1,2048,512]{2,1,0:T(8,128)(2,1)} %param.30, bf16[128,8,2048]{2,1,0:T(8,128)(2,1)} %copy-done.4), kind=kOutput, calls=%fused_computation.8 | convolution fusion | flops 4300210176 | bytes 14680064 | tf_op jit(solution)/shard_map/dot_general | solution.py:87
  114.7 0.0 copy-start.7
  114.7 5.6 %all-to-all-start.2 = ((bf16[128,8,2048]{2,1,0:T(8,128)(2,1)}), bf16[128,8,2048]{2,1,0:T(8,128)(2,1)}, u32[]{:S(2)}, u32[]{:S(2)}) async-start(bf16[128,8,2048]{2,1,0:T(8,128)(2,1)} %convert_bitcast_fusion), calls=%async_computation.2 | async-start | bytes 8388608 | tf_op jit(solution)/shard_map/all_to_all | solution.py:90
  120.3 0.0 copy-done.7
  120.3 0.1 copy.37
  120.5 0.0 copy-done.3
  120.5 2.0 %fusion.50 = f32[128,512]{1,0:T(8,128)S(1)} fusion(bf16[128,2048]{1,0:T(8,128)(2,1)S(1)} %multiply_convert_fusion.1, bf16[2048,512]{1,0:T(8,128)(2,1)} %param.26), kind=kOutput, calls=%fused_computation.76 | convolution fusion | flops 268435456 | bytes 2883584 | tf_op jit(solution)/shard_map/dot_general | solution.py:21
  122.5 50.6 %all-to-all-done.2 = bf16[128,8,2048]{2,1,0:T(8,128)(2,1)} async-done(((bf16[128,8,2048]{2,1,0:T(8,128)(2,1)}), bf16[128,8,2048]{2,1,0:T(8,128)(2,1)}, u32[]{:S(2)}, u32[]{:S(2)}) %all-to-all-start.2) | async-done | bytes 4194336 | tf_op jit(solution)/shard_map/all_to_all | solution.py:90
  173.2 9.8 %gather_fusion.1 = bf16[768,2048]{1,0:T(8,128)(2,1)} fusion(bf16[1024,2048]{1,0:T(8,128)(2,1)} %bitcast.14, s32[1024]{0:T(1024)S(1)} %pad_clamp_fusion), kind=kCustom, calls=%fused_computation.1 | custom fusion | bytes 6294528 | tf_op jit(solution)/shard_map/gather | solution.py:99
  183.0 6.6 %reshape.89 = f32[128,6,2048]{2,1,0:T(8,128)} reshape(bf16[768,2048]{1,0:T(8,128)(2,1)} %gather_fusion.1) | data formatting | bytes 9437184 | tf_op jit(solution)/shard_map/convert_element_type | solution.py:99
  189.5 0.0 copy-start.2
  189.5 7.7 %multiply_reduce_fusion = f32[128,2048]{1,0:T(8,128)} fusion(f32[128,6,2048]{2,1,0:T(8,128)} %reshape.89, f32[128,6]{1,0:T(8,128)S(1)} %copy.37), kind=kLoop, calls=%fused_computation.3 | loop fusion | flops 2883584 | bytes 7343104 | tf_op jit(solution)/shard_map/reduce_sum | solution.py:102
  197.2 0.0 copy-done.2
  197.2 4.3 %fusion.6 = bf16[128,2048]{1,0:T(8,128)(2,1)} fusion(f32[128,2048]{1,0:T(8,128)} %multiply_reduce_fusion, f32[128,2048]{1,0:T(8,128)S(1)} %copy-done.2, bf16[512,2048]{1,0:T(8,128)(2,1)} %param.28, bf16[128,2048]{1,0:T(8,128)(2,1)} %copy-done.3, bf16[2048,512]{1,0:T(8,128)(2,1)} %param.27, f32[128,512]{1,0:T(8,128)S(1)} %fusion.50), kind=kOutput, calls=%fused_computation.13 | convolution fusion | flops 538050560 | bytes 7602176 | tf_op jit(solution)/shard_map/dot_general | solution.py:59
  (12 shorter events, 0.2 us)
Async XLA Ops:
  0.0 104.7 %copy-start = (bf16[1,512,2048]{2,1,0:T(8,128)(2,1)S(1)}, bf16[1,512,2048]{2,1,0:T(8,128)(2,1)}, u32[]{:S(2)}) copy-start(bf16[1,512,2048]{2,1,0:T(8,128)(2,1)} %param.31) | copy-start | bytes 6291460
  2.1 7.9 %collective-permute-start = (f32[2,192]{0,1:T(8,128)}, f32[2,192]{0,1:T(8,128)}, u32[]{:S(2)}, u32[]{:S(2)}) collective-permute-start(f32[2,192]{0,1:T(8,128)} %slice.36), channel_id=1, source_target_pairs={{0,8},{8,16},{16,24},{24,32},{32,40},{40,48},{48,56},{56,64},{64,7... | collective-permute-start | bytes 4616 | tf_op jit(solution)/shard_map/ppermute | solution.py:10
  9.6 1.0 copy-start.6
  9.6 16.6 %copy-start.8 = (f32[1536]{0:T(1024)S(1)}, f32[1536]{0:T(1024)}, u32[]{:S(2)}) copy-start(f32[1536]{0:T(1024)} %param.20) | copy-start | bytes 18436
  9.7 16.8 %copy-start.5 = (bf16[128,2048]{1,0:T(8,128)(2,1)S(1)}, bf16[128,2048]{1,0:T(8,128)(2,1)}, u32[]{:S(2)}) copy-start(bf16[128,2048]{1,0:T(8,128)(2,1)} %param.22) | copy-start | bytes 1572868
  12.9 13.1 %all-to-all-start = ((bf16[8,128,192]{1,2,0:T(8,128)(2,1)}), bf16[8,128,192]{1,2,0:T(8,128)(2,1)S(1)}, u32[]{:S(2)}, u32[]{:S(2)}) async-start(bf16[8,128,192]{1,2,0:T(8,128)(2,1)} %copy_bitcast_fusion), calls=%async_computation | async-start | bytes 786432 | tf_op jit(solution)/shard_map/all_to_all | solution.py:54
  26.5 4.9 %copy-start.9 = (f32[2048]{0:T(1024)S(1)}, f32[2048]{0:T(1024)}, u32[]{:S(2)}) copy-start(f32[2048]{0:T(1024)} %param.23) | copy-start | bytes 24580
  30.4 1.0 copy-start.1
  31.6 88.9 %copy-start.3 = (bf16[128,2048]{1,0:T(8,128)(2,1)}, bf16[128,2048]{1,0:T(8,128)(2,1)S(1)}, u32[]{:S(2)}) copy-start(bf16[128,2048]{1,0:T(8,128)(2,1)S(1)} %multiply_convert_fusion.1) | copy-start | bytes 1572868
  37.7 63.3 %copy-start.10 = (bf16[1,2048,512]{2,1,0:T(8,128)(2,1)S(1)}, bf16[1,2048,512]{2,1,0:T(8,128)(2,1)}, u32[]{:S(2)}) copy-start(bf16[1,2048,512]{2,1,0:T(8,128)(2,1)} %param.29) | copy-start | bytes 6291460
  99.0 2.0 copy-start.4
  114.7 5.6 %copy-start.7 = (f32[128,6]{0,1:T(8,128)S(1)}, f32[128,6]{0,1:T(8,128)}, u32[]{:S(2)}) copy-start(f32[128,6]{0,1:T(8,128)} %param.25) | copy-start | bytes 9220
  114.7 58.5 %all-to-all-start.2 = ((bf16[128,8,2048]{2,1,0:T(8,128)(2,1)}), bf16[128,8,2048]{2,1,0:T(8,128)(2,1)}, u32[]{:S(2)}, u32[]{:S(2)}) async-start(bf16[128,8,2048]{2,1,0:T(8,128)(2,1)} %convert_bitcast_fusion), calls=%async_computation.2 | async-start | bytes 8388608 | tf_op jit(solution)/shard_map/all_to_all | solution.py:90
  189.5 7.7 %copy-start.2 = (f32[128,2048]{1,0:T(8,128)S(1)}, f32[128,2048]{1,0:T(8,128)}, u32[]{:S(2)}) copy-start(f32[128,2048]{1,0:T(8,128)} %copy-done.1) | copy-start | bytes 3145732
where the time goes:
time: 202 us
  blocking collectives  61.4 us (30%)
  waiting for transfers between devices  54.6 us (27%)
  local copies, waits for them, and re-layouts  32.5 us (16%)
  matrix products  23.9 us (12%)
  starting transfers between devices  15.6 us (8%)
  other arithmetic  13.3 us (7%)
    all_to_all x1, blocking collectives, body(): lax.all_to_all(outgoing, ('sp', 'tp'), split_axis=0, concat_axis=0, tiled...  61.4 us
    all_to_all x1, waiting for transfers between devices, body(): lax.all_to_all(result.reshape(leading + (model_width,)), ('sp', 'tp'), sp...  50.6 us
    dot_general x1, matrix products, body(): jnp.dot(hidden, expert_down[0], preferred_element_type=jnp.float32)  9.96 us
    gather x1, local copies, waits for them, and re-layouts, body(): flat_returned[slot_index].reshape(row_count, top_count, model_width)  9.82 us
    reduce_sum x1, other arithmetic, body(): routed = jnp.sum(picked * gate_values[:, :, None], axis=1)  7.69 us
    convert_element_type x1, local copies, waits for them, and re-layouts, body(): flat_returned[slot_index].reshape(row_count, top_count, model_width)  6.55 us
    gather x1, local copies, waits for them, and re-layouts, body(): outgoing = padded[source_rows].reshape(experts_total, capacity, model_width)  6.02 us
    dot_general x2, matrix products, swiglu_hidden(): jnp.dot(row_block, weight_gate, preferred_element_type=jnp.float32)  5.76 us
  transfers between devices with their start and end apart: 3, of which 2 were waited for; matrix products, arithmetic and copies ran while one was open for 5% of the time, Pallas kernels for 0%

commit v1 on v0

--- a/solution.py
+++ b/solution.py
@@ -67,20 +67,21 @@
     experts_total = sp_count * tp_count
     top_count = routes.shape[1]
     capacity = max(2, 4 * row_count * top_count // (3 * experts_total))
-    flat_ids = routes.reshape(-1)
-    onehot = (flat_ids[:, None] == jnp.arange(experts_total, dtype=jnp.int32)[None, :]).astype(
-        jnp.int32
-    )
-    before = jnp.cumsum(onehot, axis=0) - onehot
-    slot_rank = jnp.sum(before * onehot, axis=1)
-    slot_index = flat_ids * capacity + slot_rank
-    source_rows = (
-        jnp.full((experts_total * capacity,), row_count, jnp.int32)
-        .at[slot_index]
-        .set(jnp.arange(flat_ids.shape[0], dtype=jnp.int32) // top_count)
-    )
-    padded = jnp.concatenate([normed, jnp.zeros((1, model_width), jnp.bfloat16)], axis=0)
-    outgoing = padded[source_rows].reshape(experts_total, capacity, model_width)
+    expert_ids = jnp.arange(experts_total, dtype=jnp.int32)
+    named = routes.T[:, None, :] == expert_ids[None, :, None]
+    mask = jnp.sum(named.astype(jnp.float32), axis=0)
+    earlier_rows = jnp.triu(jnp.ones((row_count, row_count), jnp.bfloat16), 1)
+    rank = jnp.dot(mask.astype(jnp.bfloat16), earlier_rows, preferred_element_type=jnp.float32)
+    gate_values = route_weights / jnp.sum(route_weights, axis=1, keepdims=True) * 2.5
+    gates = jnp.sum(jnp.where(named, gate_values.T[:, None, :], 0.0), axis=0)
+    slot_ranks = jnp.arange(capacity, dtype=jnp.float32)[None, :, None]
+    chosen = (rank[:, None, :] == slot_ranks) & (mask[:, None, :] > 0)
+    select = chosen.astype(jnp.bfloat16).reshape(experts_total * capacity, row_count)
+    weight = jnp.where(chosen, gates[:, None, :], 0.0).reshape(experts_total * capacity, row_count)
+    weight_high = weight.astype(jnp.bfloat16)
+    weight_low = (weight - weight_high.astype(jnp.float32)).astype(jnp.bfloat16)
+    outgoing = jnp.dot(select, normed, preferred_element_type=jnp.float32).astype(jnp.bfloat16)
+    outgoing = outgoing.reshape(experts_total, capacity, model_width)
     arrived = lax.all_to_all(outgoing, ("sp", "tp"), split_axis=0, concat_axis=0, tiled=True)
     leading = arrived.shape[:-1]
     hidden = swiglu_hidden(arrived.reshape(-1, model_width), expert_gate[0], expert_up[0])
@@ -95,11 +96,12 @@
         tiled=True,
     )
     flat_returned = returned_rows.reshape(experts_total * capacity, model_width)
-    picked = (
-        flat_returned[slot_index].reshape(row_count, top_count, model_width).astype(jnp.float32)
+    transposed = (((0,), (0,)), ((), ()))
+    routed = lax.dot_general(
+        weight_high, flat_returned, transposed, preferred_element_type=jnp.float32
+    ) + lax.dot_general(
+        weight_low, flat_returned, transposed, preferred_element_type=jnp.float32
     )
-    gate_values = route_weights / jnp.sum(route_weights, axis=1, keepdims=True) * 2.5
-    routed = jnp.sum(picked * gate_values[:, :, None], axis=1)
     return (stream + shared_result + routed).astype(jnp.bfloat16)
 
 

time: 202 us -> 178 us (0.88)
  local copies, waits for them, and re-layouts: 32.5 us -> 2.99 us
  matrix products: 23.9 us -> 32.3 us
  other arithmetic: 13.3 us -> 6.38 us
  waiting for transfers between devices: 54.6 us -> 58.3 us
    gather x2 -> x0, local copies, waits for them, and re-layouts: 15.8 us -> none  [the longest x1 9.82 us: body(): flat_returned[slot_index].reshape(row_count, top_count, model_width)]
    dot_general x0 -> x4, matrix products: none -> 8.39 us  [the longest x1 3.96 us: body(): lax.dot_general(weight_high, flat_returned, transposed, preferred_element...]
    reduce_sum x2 -> x1, other arithmetic: 7.99 us -> 0.77 us  [body(): gates = jnp.sum(jnp.where(named, gate_values.T[:, None, :], 0.0), axis=0)]
    convert_element_type x1 -> x0, local copies, waits for them, and re-layouts: 6.55 us -> none  [body(): flat_returned[slot_index].reshape(row_count, top_count, model_width)]
    all_to_all x1, waiting for transfers between devices: 4.01 us -> 7.55 us  [body(): lax.all_to_all(conv_out, 'tp', split_axis=0, concat_axis=1, tiled=True)]
    scatter x1 -> x0, local copies, waits for them, and re-layouts: 3.38 us -> none  [body(): source_rows = jnp.full((experts_total * capacity,), row_count, jnp.int32)...]
    unnamed x23 -> x12, local copies, waits for them, and re-layouts: 4.29 us -> 2 us
  transfers between devices with their start and end apart: 3 -> 3, of which waited for: 2 -> 2; matrix products, arithmetic and copies ran while one was open for 5% -> 3% of each run, Pallas kernels for 0% -> 0%
where the time goes in v1:
time: 178 us; the launch traced here: 177 us
  blocking collectives  62.1 us (35%)
  waiting for transfers between devices  58.3 us (33%)
  matrix products  32.3 us (18%)
  starting transfers between devices  14.9 us (8%)
  other arithmetic  6.38 us (4%)
  local copies, waits for them, and re-layouts  2.99 us (2%)
    all_to_all x1, blocking collectives, body(): lax.all_to_all(outgoing, ('sp', 'tp'), split_axis=0, concat_axis=0, tiled...  62.1 us
    all_to_all x1, waiting for transfers between devices, body(): lax.all_to_all(result.reshape(leading + (model_width,)), ('sp', 'tp'), sp...  50.7 us
    dot_general x1, matrix products, body(): jnp.dot(hidden, expert_down[0], preferred_element_type=jnp.float32)  9.96 us
    all_to_all x1, waiting for transfers between devices, body(): lax.all_to_all(conv_out, 'tp', split_axis=0, concat_axis=1, tiled=True)  7.55 us
    dot_general x2, matrix products, swiglu_hidden(): jnp.dot(row_block, weight_gate, preferred_element_type=jnp.float32)  5.81 us
    all_to_all x1, starting transfers between devices, body(): lax.all_to_all(result.reshape(leading + (model_width,)), ('sp', 'tp'), sp...  5.5 us
    all_to_all x1, starting transfers between devices, body(): lax.all_to_all(conv_out, 'tp', split_axis=0, concat_axis=1, tiled=True)  5.42 us
    dot_general x1, matrix products, body(): jnp.dot(swiglu_hidden(normed, shared_gate, shared_up), shared_down, prefe...  4.19 us
  transfers between devices with their start and end apart: 3, of which 2 were waited for; matrix products, arithmetic and copies ran while one was open for 3% of the time, Pallas kernels for 0%

profile of v1, /device:TPU:1, one launch (start us, length us, event | category | flops | bytes accessed | tf_op | source)
XLA Modules:
  0.0 177.1 jit_solution(12434396145566647151)
XLA Ops:
  0.0 0.0 copy-start
  0.0 1.4 convert_multiply_fusion
  1.4 0.0 copy-start.3
  1.4 0.1 slice.24
  1.5 3.9 %collective-permute-start = (f32[2,192]{0,1:T(8,128)S(1)}, f32[2,192]{0,1:T(8,128)S(1)}, u32[]{:S(2)}, u32[]{:S(2)}) collective-permute-start(f32[2,192]{0,1:T(8,128)S(1)} %slice.24), channel_id=1, source_target_pairs={{0,8},{8,16},{16,24},{24,32},{32,40},{40,48},{48,56},{56,64},{64,7... | collective-permute-start | bytes 4616 | tf_op jit(solution)/shard_map/ppermute | solution.py:10
  5.4 0.8 fusion.66
  6.2 0.7 reduce_sum.48
  6.9 0.7 multiply_bitcast_fusion
  7.6 0.8 select_reduce_fusion
  8.4 0.1 eq.48
  8.5 0.0 collective-permute-done
  8.5 2.3 %copy_bitcast_fusion = bf16[8,128,192]{1,2,0:T(8,128)(2,1)} fusion(f32[1024,192]{0,1:T(8,128)S(1)} %convert_multiply_fusion, f32[192]{0:T(256)S(1)} %bitcast.68, f32[2,192]{0,1:T(8,128)S(1)} %collective-permute-done, f32[192]{0:T(256)S(1)} %bitcast.69, f32[192]{0:T(256)S(1)} %bitcast.67, bf16[1024,192]{0,1:T(8,128)(2,1)} %param.16), kind=kLoop, calls=%fused_computation.45 | loop fusion | flops 1966080 | bytes 1576704 | tf_op jit(solution)/shard_map/all_to_all | solution.py:54
  10.8 5.4 %all-to-all-start = ((bf16[8,128,192]{1,2,0:T(8,128)(2,1)}), bf16[8,128,192]{1,2,0:T(8,128)(2,1)S(1)}, u32[]{:S(2)}, u32[]{:S(2)}) async-start(bf16[8,128,192]{1,2,0:T(8,128)(2,1)} %copy_bitcast_fusion), calls=%async_computation | async-start | bytes 786432 | tf_op jit(solution)/shard_map/all_to_all | solution.py:54
  16.3 0.1 fusion.54
  16.4 7.6 %all-to-all-done = bf16[8,128,192]{1,2,0:T(8,128)(2,1)S(1)} async-done(((bf16[8,128,192]{1,2,0:T(8,128)(2,1)}), bf16[8,128,192]{1,2,0:T(8,128)(2,1)S(1)}, u32[]{:S(2)}, u32[]{:S(2)}) %all-to-all-start) | async-done | bytes 393248 | tf_op jit(solution)/shard_map/all_to_all | solution.py:54
  24.0 0.2 multiply_reduce_fusion.1
  24.2 0.0 copy-done.3
  24.2 0.3 fusion.28
  24.5 0.0 copy-start.2
  24.5 4.0 %multiply_reduce_fusion = (f32[128]{0:T(128)S(1)}, f32[128,2048]{1,0:T(8,128)S(1)}) fusion(f32[128]{0:T(128)S(1)} %add_rsqrt_fusion.1, bf16[128,1536]{0,1:T(8,128)(2,1)S(1)} %fusion.28, bf16[1536,2048]{1,0:T(8,128)(2,1)} %param.21, bf16[128,2048]{1,0:T(8,128)(2,1)} %param.22), kind=kOutput, calls=%fused_computation.22 | convolution fusion | flops 806616960 | bytes 8258560 | tf_op jit(solution)/shard_map/dot_general | solution.py:17
  28.5 0.0 copy-start.4
  28.5 0.0 copy-done.2
  28.5 1.3 convert_bitcast_fusion.1
  29.8 0.0 copy-done.4
  29.9 0.0 copy-start.5
  29.9 62.1 %all_to_all.23 = bf16[128,8,2048]{2,1,0:T(8,128)(2,1)S(1)} all-to-all(bf16[128,8,2048]{2,1,0:T(8,128)(2,1)S(1)} %convert_bitcast_fusion.1), channel_id=1, replica_groups=mesh['sp'=16,'tp'=8] {'sp','tp'}, dimensions={0} | all-to-all | bytes 8388608 | tf_op jit(solution)/shard_map/all_to_all | solution.py:85
  91.9 0.0 copy-start.1
  91.9 2.0 %copy-done.1 = bf16[128,8,2048]{2,1,0:T(8,128)(2,1)} copy-done((bf16[128,8,2048]{2,1,0:T(8,128)(2,1)}, bf16[128,8,2048]{2,1,0:T(8,128)(2,1)S(1)}, u32[]{:S(2)}) %copy-start.1) | copy-done | bytes 4194328
  93.9 0.0 copy-done.5
  93.9 3.7 %fusion.2 = f32[1024,512]{1,0:T(8,128)} fusion(bf16[128,8,2048]{2,1,0:T(8,128)(2,1)S(1)} %all_to_all.23, bf16[1,2048,512]{2,1,0:T(8,128)(2,1)S(1)} %copy-done.5), kind=kOutput, calls=%fused_computation.2 | convolution fusion | flops 2147483648 | bytes 8388608 | tf_op jit(solution)/shard_map/dot_general | solution.py:21
  97.6 0.0 copy-done
  97.6 10.0 %convert_bitcast_fusion = bf16[128,8,2048]{2,1,0:T(8,128)(2,1)} fusion(bf16[1,512,2048]{2,1,0:T(8,128)(2,1)S(1)} %copy-done, f32[1024,512]{1,0:T(8,128)} %fusion.2, bf16[1,2048,512]{2,1,0:T(8,128)(2,1)} %param.30, bf16[128,8,2048]{2,1,0:T(8,128)(2,1)} %copy-done.1), kind=kOutput, calls=%fused_computation.4 | convolution fusion | flops 4300210176 | bytes 14680064 | tf_op jit(solution)/shard_map/dot_general | solution.py:88
  107.6 5.5 %all-to-all-start.2 = ((bf16[128,8,2048]{2,1,0:T(8,128)(2,1)}), bf16[128,8,2048]{2,1,0:T(8,128)(2,1)}, u32[]{:S(2)}, u32[]{:S(2)}) async-start(bf16[128,8,2048]{2,1,0:T(8,128)(2,1)} %convert_bitcast_fusion), calls=%async_computation.2 | async-start | bytes 8388608 | tf_op jit(solution)/shard_map/all_to_all | solution.py:91
  113.1 2.1 %fusion.65 = f32[128,512]{1,0:T(8,128)S(1)} fusion(bf16[2048,512]{1,0:T(8,128)(2,1)} %param.26, f32[128,2048]{1,0:T(8,128)S(1)} %get-tuple-element.11, f32[2048]{0:T(1024)} %param.23, f32[128]{0:T(128)} %copy-done.4), kind=kOutput, calls=%fused_computation.83 | convolution fusion | flops 269221888 | bytes 3416576 | tf_op jit(solution)/shard_map/dot_general | solution.py:21
  115.2 50.7 %all-to-all-done.2 = bf16[128,8,2048]{2,1,0:T(8,128)(2,1)} async-done(((bf16[128,8,2048]{2,1,0:T(8,128)(2,1)}), bf16[128,8,2048]{2,1,0:T(8,128)(2,1)}, u32[]{:S(2)}, u32[]{:S(2)}) %all-to-all-start.2) | async-done | bytes 4194336 | tf_op jit(solution)/shard_map/all_to_all | solution.py:91
  165.9 3.0 %convolution_bitcast_fusion = f32[128,2048]{1,0:T(8,128)S(1)} fusion(bf16[128,8,2048]{2,1,0:T(8,128)(2,1)} %all-to-all-done.2, f32[128,128]{1,0:T(8,128)S(1)} %get-tuple-element.5, f32[128,128]{1,0:T(8,128)S(1)} %fusion.54, pred[128,128]{1,0:T(8,128)(4,1)S(1)} %broadcast_compare_fusion), kind=kOutput, calls=%fused_computation.7 | convolution fusion | flops 537788416 | bytes 5390336 | tf_op jit(solution)/shard_map/dot_general | solution.py:102
  168.9 4.0 %fusion.6 = f32[128,2048]{1,0:T(8,128)} fusion(f32[128,2048]{1,0:T(8,128)S(1)} %convolution_bitcast_fusion, bf16[128,8,2048]{2,1,0:T(8,128)(2,1)} %all-to-all-done.2, f32[128,128]{1,0:T(8,128)S(1)} %get-tuple-element.5, f32[128,128]{1,0:T(8,128)S(1)} %fusion.54, pred[128,128]{1,0:T(8,128)(4,1)S(1)} %broadcast_compare_fusion), kind=kOutput, calls=%fused_computation.12 | convolution fusion | flops 537526272 | bytes 6438912 | tf_op jit(solution)/shard_map/dot_general | solution.py:100
  172.9 4.2 %fusion.7 = bf16[128,2048]{1,0:T(8,128)(2,1)} fusion(f32[128,2048]{1,0:T(8,128)} %fusion.6, f32[128,2048]{1,0:T(8,128)S(1)} %get-tuple-element.11, bf16[512,2048]{1,0:T(8,128)(2,1)} %param.28, bf16[2048,512]{1,0:T(8,128)(2,1)} %param.27, f32[128,512]{1,0:T(8,128)S(1)} %fusion.65, f32[2048]{0:T(1024)} %param.23, f32[128]{0:T(128)} %copy-done.4), kind=kOutput, calls=%fused_computation.13 | convolution fusion | flops 538836992 | bytes 7086592 | tf_op jit(solution)/shard_map/dot_general | solution.py:59
  (4 shorter events, 0.0 us)
Async XLA Ops:
  0.0 97.6 %copy-start = (bf16[1,512,2048]{2,1,0:T(8,128)(2,1)S(1)}, bf16[1,512,2048]{2,1,0:T(8,128)(2,1)}, u32[]{:S(2)}) copy-start(bf16[1,512,2048]{2,1,0:T(8,128)(2,1)} %param.31) | copy-start | bytes 6291460
  1.4 22.8 %copy-start.3 = (f32[1536]{0:T(1024)S(1)}, f32[1536]{0:T(1024)}, u32[]{:S(2)}) copy-start(f32[1536]{0:T(1024)} %param.20) | copy-start | bytes 18436
  1.5 7.0 %collective-permute-start = (f32[2,192]{0,1:T(8,128)S(1)}, f32[2,192]{0,1:T(8,128)S(1)}, u32[]{:S(2)}, u32[]{:S(2)}) collective-permute-start(f32[2,192]{0,1:T(8,128)S(1)} %slice.24), channel_id=1, source_target_pairs={{0,8},{8,16},{16,24},{24,32},{32,40},{40,48},{48,56},{56,64},{64,7... | collective-permute-start | bytes 4616 | tf_op jit(solution)/shard_map/ppermute | solution.py:10
  10.8 13.1 %all-to-all-start = ((bf16[8,128,192]{1,2,0:T(8,128)(2,1)}), bf16[8,128,192]{1,2,0:T(8,128)(2,1)S(1)}, u32[]{:S(2)}, u32[]{:S(2)}) async-start(bf16[8,128,192]{1,2,0:T(8,128)(2,1)} %copy_bitcast_fusion), calls=%async_computation | async-start | bytes 786432 | tf_op jit(solution)/shard_map/all_to_all | solution.py:54
  24.5 4.0 %copy-start.2 = (f32[2048]{0:T(1024)S(1)}, f32[2048]{0:T(1024)}, u32[]{:S(2)}) copy-start(f32[2048]{0:T(1024)} %param.23) | copy-start | bytes 24580
  28.5 1.4 copy-start.4
  29.9 64.1 %copy-start.5 = (bf16[1,2048,512]{2,1,0:T(8,128)(2,1)S(1)}, bf16[1,2048,512]{2,1,0:T(8,128)(2,1)}, u32[]{:S(2)}) copy-start(bf16[1,2048,512]{2,1,0:T(8,128)(2,1)} %param.29) | copy-start | bytes 6291460
  91.9 2.0 %copy-start.1 = (bf16[128,8,2048]{2,1,0:T(8,128)(2,1)}, bf16[128,8,2048]{2,1,0:T(8,128)(2,1)S(1)}, u32[]{:S(2)}) copy-start(bf16[128,8,2048]{2,1,0:T(8,128)(2,1)S(1)} %all_to_all.23) | copy-start | bytes 12582916
  107.6 58.4 %all-to-all-start.2 = ((bf16[128,8,2048]{2,1,0:T(8,128)(2,1)}), bf16[128,8,2048]{2,1,0:T(8,128)(2,1)}, u32[]{:S(2)}, u32[]{:S(2)}) async-start(bf16[128,8,2048]{2,1,0:T(8,128)(2,1)} %convert_bitcast_fusion), calls=%async_computation.2 | async-start | bytes 8388608 | tf_op jit(solution)/shard_map/all_to_all | solution.py:91

commit v2 on v0

--- a/solution.py
+++ b/solution.py
@@ -1,7 +1,301 @@
 import jax
 import jax.numpy as jnp
+import numpy as np
 from jax import lax
+from jax.experimental import pallas as pl
+from jax.experimental.pallas import tpu as pltpu
 from jax.sharding import PartitionSpec as P
+
+
+COLORS = (("z", "x", "y", 0, 640), ("x", "y", "z", 640, 640), ("y", "z", "x", 1280, 768))
+AXES = ("z", "x", "y")
+RING = 4
+CORES = 2
+SLOTS = 8
+MESH = pl.DeviceIdType.MESH
+PAIRS = tuple((g, h) for g in range(RING) for h in range(CORES) if (g, h) != (0, 0))
+NEAR_FIRST = (1, 3, 2)
+
+
+def expansion_table(experts_total):
+    slot = np.arange(experts_total * SLOTS)
+    ids = []
+    for first, second, third, _, _ in COLORS:
+        digits = {
+            first: slot // (RING * RING * CORES * SLOTS) % RING,
+            second: slot // (RING * CORES * SLOTS) % RING,
+            third: slot // (CORES * SLOTS) % RING,
+        }
+        core = slot // SLOTS % CORES
+        ids.append(((digits["z"] * RING + digits["x"]) * RING + digits["y"]) * CORES + core)
+    return np.concatenate(ids)
+
+
+def slot_tables(routes, route_weights, experts_total):
+    row_count = routes.shape[0]
+    expert_ids = jnp.arange(experts_total, dtype=jnp.int32)
+    gate_values = route_weights / jnp.sum(route_weights, axis=1, keepdims=True) * 2.5
+    named = routes[:, :, None] == expert_ids[None, None, :]
+    mask = jnp.sum(named.astype(jnp.float32), axis=1)
+    gates = jnp.sum(jnp.where(named, gate_values[:, :, None], 0.0), axis=1)
+    earlier = jnp.tril(jnp.ones((row_count, row_count), jnp.bfloat16), -1)
+    rank = jnp.dot(earlier, mask.astype(jnp.bfloat16), preferred_element_type=jnp.float32)
+    ranks = jnp.arange(SLOTS, dtype=jnp.float32)[:, None, None]
+    chosen = (rank[None] == ranks) & (mask[None] > 0)
+    numbers = jnp.arange(1, row_count + 1, dtype=jnp.float32)[None, :, None]
+    token = jnp.sum(jnp.where(chosen, numbers, 0.0), axis=1)
+    gate = jnp.sum(jnp.where(chosen, gates[None], 0.0), axis=1)
+    high = gate.astype(jnp.bfloat16)
+    low = (gate - high.astype(jnp.float32)).astype(jnp.bfloat16)
+    stacked = jnp.concatenate([token.astype(jnp.bfloat16), high, low], axis=0)
+    ids = jnp.asarray(expansion_table(experts_total), jnp.int32)
+    expand = (expert_ids[:, None] == ids[None, :]).astype(jnp.bfloat16)
+    spread = jnp.dot(stacked, expand, preferred_element_type=jnp.float32)
+    slot_rank = jnp.arange(ids.shape[0], dtype=jnp.int32) % SLOTS
+    keep = jnp.arange(SLOTS, dtype=jnp.int32)[:, None] == slot_rank[None, :]
+    rows = jnp.sum(jnp.where(keep[None], spread.reshape(3, SLOTS, -1), 0.0), axis=1)
+    rows = rows.reshape(3, len(COLORS), RING, -1).transpose(1, 2, 0, 3)
+    return jnp.pad(rows, ((0, 0), (0, 0), (0, SLOTS - 3), (0, 0)))
+
+
+def moe_kernel(
+    normed, tables, base, w_gate, w_up, w_down, out,
+    v_gate, v_up, v_down, seen_tab, arrived, result, total, own_part,
+    ag0, ag1, ag2, pick0, pick1, pick2, mid0, mid1, mid2,
+    back0, back1, back2, slots0, slots1, slots2, part0, part1, part2, got0, got1, got2,
+    w_sem, tab_s, tab_r, ag_s, ag_r, p2_s, p2_r, p3_s, p3_r, r1_s, r1_r, r2_s, r2_r, r3_s, r3_r,
+):
+    ag, pick, mid = (ag0, ag1, ag2), (pick0, pick1, pick2), (mid0, mid1, mid2)
+    back, slots = (back0, back1, back2), (slots0, slots1, slots2)
+    part, got = (part0, part1, part2), (got0, got1, got2)
+    sp, tp = lax.axis_index("sp"), lax.axis_index("tp")
+    at = {"z": sp // RING, "x": sp % RING, "y": tp // CORES}
+    core = tp % CORES
+
+    def device(core_step=0, **steps):
+        p = {k: (at[k] + steps.get(k, 0)) % RING for k in AXES}
+        return (p["z"] * RING + p["x"], p["y"] * CORES + (core + core_step) % CORES)
+
+    def send(src, dst, s, r, target):
+        copy = pltpu.make_async_remote_copy(
+            src_ref=src, dst_ref=dst, send_sem=s, recv_sem=r, device_id=target, device_id_type=MESH
+        )
+        copy.start()
+        return copy
+
+    def lead(q, i, d):
+        return (d, i) if q == 2 else (i, d)
+
+    def piece(ref, q, g, h):
+        c0, w = COLORS[q][3:]
+        cols = pl.ds(c0, w)
+        if q == 0:
+            return ref.at[:, :, g, h, :, cols]
+        if q == 1:
+            return ref.at[g, :, :, h, :, cols]
+        return ref.at[:, g, :, h, :, cols]
+
+    loads = [
+        pltpu.make_async_copy(src, dst, w_sem.at[n])
+        for n, (src, dst) in enumerate(((w_gate, v_gate), (w_up, v_up), (w_down, v_down)))
+    ]
+    for load in loads:
+        load.start()
+
+    barrier = pltpu.get_barrier_semaphore()
+    peers = [device(1)] + [
+        device(h, **{axis: g}) for axis in AXES for g in range(1, RING) for h in range(CORES)
+    ]
+    for peer in peers:
+        pl.semaphore_signal(barrier, inc=1, device_id=peer, device_id_type=MESH)
+    pl.semaphore_wait(barrier, len(peers))
+
+    sent = []
+    ag_copy, tab_copy = {}, {}
+    for d in NEAR_FIRST:
+        for q, (first, _, _, c0, w) in enumerate(COLORS):
+            target = device(**{first: d})
+            tab_copy[q, d] = send(
+                tables.at[q, (at[first] + d) % RING], seen_tab.at[q, d - 1],
+                tab_s.at[q, d - 1], tab_r.at[q, d - 1], target,
+            )
+            ag_copy[q, d] = send(
+                normed.at[:, pl.ds(c0, w)], ag[q].at[d - 1],
+                ag_s.at[q, d - 1], ag_r.at[q, d - 1], target,
+            )
+            sent += [tab_copy[q, d], ag_copy[q, d]]
+
+    row_count = normed.shape[0]
+    group = RING * CORES * SLOTS
+    numbers = (lax.broadcasted_iota(jnp.int32, (row_count, RING * group), 0) + 1).astype(jnp.float32)
+
+    def table(q, i):
+        return tables[q, at[COLORS[q][0]]] if i == 0 else seen_tab[q, i - 1]
+
+    p2_copy = {}
+    for i in (0,) + NEAR_FIRST:
+        for q, (_, second, _, c0, w) in enumerate(COLORS):
+            if i == 0:
+                rows = normed[:, c0 : c0 + w]
+            else:
+                tab_copy[q, i].wait_recv()
+                ag_copy[q, i].wait_recv()
+                rows = ag[q][i - 1]
+            onehot = (numbers == table(q, i)[0:1, :]).astype(jnp.bfloat16)
+            picked = lax.dot_general(
+                onehot, rows, (((0,), (0,)), ((), ())), preferred_element_type=jnp.float32
+            )
+            picked = picked.astype(jnp.bfloat16).reshape(RING, RING * CORES, SLOTS, w)
+            for b in range(RING):
+                pick[q][b, i] = picked[b]
+            for d in NEAR_FIRST:
+                copy = send(
+                    pick[q].at[(at[second] + d) % RING, i], mid[q].at[lead(q, i, d)],
+                    p2_s.at[q, d - 1, i], p2_r.at[q, d - 1, i], device(**{second: d}),
+                )
+                p2_copy[q, d, i] = copy
+                sent.append(copy)
+            mid[q][lead(q, i, 0)] = pick[q][at[second], i]
+
+    p3_copy = {}
+    for q, (_, _, third, c0, w) in enumerate(COLORS):
+        for i in (0,) + NEAR_FIRST:
+            for d in NEAR_FIRST:
+                p2_copy[q, d, i].wait_recv()
+        for n, (g, h) in enumerate(PAIRS):
+            k = (at[third] + g) % RING * CORES + (core + h) % CORES
+            copy = send(
+                mid[q].at[:, :, k], piece(arrived, q, g, h),
+                p3_s.at[q, n], p3_r.at[q, n], device(h, **{third: g}),
+            )
+            p3_copy[q, n] = copy
+            sent.append(copy)
+        piece(arrived, q, 0, 0)[...] = mid[q][:, :, at[third] * CORES + core]
+
+    for load in loads:
+        load.wait()
+    for q in range(len(COLORS)):
+        for n in range(len(PAIRS)):
+            p3_copy[q, n].wait_recv()
+
+    width = arrived.shape[-1]
+    block = RING * RING * CORES * SLOTS
+
+    @pl.loop(0, RING)
+    def _(zi):
+        rows = arrived[zi].reshape(block, width)
+        gate_part = jnp.dot(rows, v_gate[...], preferred_element_type=jnp.float32)
+        up_part = jnp.dot(rows, v_up[...], preferred_element_type=jnp.float32)
+        hidden = (gate_part / (1.0 + jnp.exp(-gate_part)) * up_part).astype(jnp.bfloat16)
+        done = jnp.dot(hidden, v_down[...], preferred_element_type=jnp.float32)
+        result[zi] = done.astype(jnp.bfloat16).reshape(RING, RING, CORES, SLOTS, width)
+
+    r1_copy = {}
+    for n, (g, h) in enumerate(PAIRS):
+        for q, (_, _, third, c0, w) in enumerate(COLORS):
+            copy = send(
+                piece(result, q, g, h), back[q].at[:, :, at[third] * CORES + core],
+                r1_s.at[q, n], r1_r.at[q, n], device(-h, **{third: -g}),
+            )
+            r1_copy[q, n] = copy
+            sent.append(copy)
+    r2_copy = {}
+    for q, (_, second, third, c0, w) in enumerate(COLORS):
+        back[q][:, :, at[third] * CORES + core] = piece(result, q, 0, 0)[...]
+        for n in range(len(PAIRS)):
+            r1_copy[q, n].wait_recv()
+        for d in NEAR_FIRST:
+            src = back[q].at[d] if q == 2 else back[q].at[:, d]
+            copy = send(
+                src, slots[q].at[:, at[second]],
+                r2_s.at[q, d - 1], r2_r.at[q, d - 1], device(**{second: -d}),
+            )
+            r2_copy[q, d] = copy
+            sent.append(copy)
+        slots[q][:, at[second]] = back[q][0] if q == 2 else back[q][:, 0]
+    r3_copy = {}
+    for q, (first, _, _, c0, w) in enumerate(COLORS):
+        for d in NEAR_FIRST:
+            r2_copy[q, d].wait_recv()
+        for i in NEAR_FIRST + (0,):
+            rows = slots[q][i].reshape(RING * group, w)
+            tab = table(q, i)
+            hit = numbers == tab[0:1, :]
+            high = jnp.where(hit, tab[1:2, :], 0.0).astype(jnp.bfloat16)
+            low = jnp.where(hit, tab[2:3, :], 0.0).astype(jnp.bfloat16)
+            some = jnp.dot(high, rows, preferred_element_type=jnp.float32) + jnp.dot(
+                low, rows, preferred_element_type=jnp.float32
+            )
+            if i == 0:
+                own_part[:, c0 : c0 + w] = some
+            else:
+                part[q][i - 1] = some.astype(jnp.bfloat16)
+                copy = send(
+                    part[q].at[i - 1], got[q].at[i - 1],
+                    r3_s.at[q, i - 1], r3_r.at[q, i - 1], device(**{first: -i}),
+                )
+                r3_copy[q, i] = copy
+                sent.append(copy)
+    for q, (_, _, _, c0, w) in enumerate(COLORS):
+        for i in NEAR_FIRST:
+            r3_copy[q, i].wait_recv()
+        some = own_part[:, c0 : c0 + w] + base[:, c0 : c0 + w]
+        for i in range(RING - 1):
+            some = some + got[q][i].astype(jnp.float32)
+        out[:, c0 : c0 + w] = some.astype(jnp.bfloat16)
+    for copy in sent:
+        copy.wait_send()
+
+
+def routed_layer(normed, tables, base, w_gate, w_up, w_down):
+    row_count, width = normed.shape
+    hidden = w_gate.shape[1]
+    bf16 = jnp.bfloat16
+    widths = [c[4] for c in COLORS]
+
+    def per_color(*shape):
+        return [pltpu.VMEM(shape + (w,), bf16) for w in widths]
+
+    dma = pltpu.SemaphoreType.DMA
+    colors = len(COLORS)
+    pairs = len(PAIRS)
+    scratch = (
+        [
+            pltpu.VMEM((width, hidden), bf16),
+            pltpu.VMEM((width, hidden), bf16),
+            pltpu.VMEM((hidden, width), bf16),
+            pltpu.VMEM((colors, RING - 1) + tables.shape[2:], jnp.float32),
+            pltpu.VMEM((RING, RING, RING, CORES, SLOTS, width), bf16),
+            pltpu.VMEM((RING, RING, RING, CORES, SLOTS, width), bf16),
+            pltpu.VMEM((SLOTS, 128), jnp.float32),
+            pltpu.VMEM((row_count, width), jnp.float32),
+        ]
+        + per_color(RING - 1, row_count)
+        + per_color(RING, RING, RING * CORES, SLOTS)
+        + per_color(RING, RING, RING * CORES, SLOTS)
+        + per_color(RING, RING, RING * CORES, SLOTS)
+        + per_color(RING, RING, RING * CORES, SLOTS)
+        + per_color(RING - 1, row_count)
+        + per_color(RING - 1, row_count)
+        + [dma((3,))]
+        + [dma((colors, RING - 1))] * 4
+        + [dma((colors, RING - 1, RING))] * 2
+        + [dma((colors, pairs))] * 4
+        + [dma((colors, RING - 1))] * 4
+    )
+    vmem = pl.BlockSpec(memory_space=pltpu.VMEM)
+    hbm = pl.BlockSpec(memory_space=pl.ANY)
+    return pl.pallas_call(
+        moe_kernel,
+        out_shape=jax.ShapeDtypeStruct((row_count, width), bf16),
+        in_specs=[vmem, vmem, vmem, hbm, hbm, hbm],
+        out_specs=vmem,
+        scratch_shapes=scratch,
+        compiler_params=pltpu.CompilerParams(
+            collective_id=0, has_side_effects=True, vmem_limit_bytes=56 * 2**20
+        ),
+        name="routed_layer",
+    )(normed, tables, base, w_gate, w_up, w_down)
 
 
 def from_behind(block, axis, distance):
@@ -61,46 +355,10 @@
         shared_down,
         preferred_element_type=jnp.float32,
     )
-    model_width = normed.shape[1]
-    sp_count = lax.axis_size("sp")
-    tp_count = lax.axis_size("tp")
-    experts_total = sp_count * tp_count
-    top_count = routes.shape[1]
-    capacity = max(2, 4 * row_count * top_count // (3 * experts_total))
-    flat_ids = routes.reshape(-1)
-    onehot = (flat_ids[:, None] == jnp.arange(experts_total, dtype=jnp.int32)[None, :]).astype(
-        jnp.int32
-    )
-    before = jnp.cumsum(onehot, axis=0) - onehot
-    slot_rank = jnp.sum(before * onehot, axis=1)
-    slot_index = flat_ids * capacity + slot_rank
-    source_rows = (
-        jnp.full((experts_total * capacity,), row_count, jnp.int32)
-        .at[slot_index]
-        .set(jnp.arange(flat_ids.shape[0], dtype=jnp.int32) // top_count)
-    )
-    padded = jnp.concatenate([normed, jnp.zeros((1, model_width), jnp.bfloat16)], axis=0)
-    outgoing = padded[source_rows].reshape(experts_total, capacity, model_width)
-    arrived = lax.all_to_all(outgoing, ("sp", "tp"), split_axis=0, concat_axis=0, tiled=True)
-    leading = arrived.shape[:-1]
-    hidden = swiglu_hidden(arrived.reshape(-1, model_width), expert_gate[0], expert_up[0])
-    result = jnp.dot(hidden, expert_down[0], preferred_element_type=jnp.float32).astype(
-        jnp.bfloat16
-    )
-    returned_rows = lax.all_to_all(
-        result.reshape(leading + (model_width,)),
-        ("sp", "tp"),
-        split_axis=0,
-        concat_axis=0,
-        tiled=True,
-    )
-    flat_returned = returned_rows.reshape(experts_total * capacity, model_width)
-    picked = (
-        flat_returned[slot_index].reshape(row_count, top_count, model_width).astype(jnp.float32)
-    )
-    gate_values = route_weights / jnp.sum(route_weights, axis=1, keepdims=True) * 2.5
-    routed = jnp.sum(picked * gate_values[:, :, None], axis=1)
-    return (stream + shared_result + routed).astype(jnp.bfloat16)
+    experts_total = lax.axis_size("sp") * lax.axis_size("tp")
+    tables = slot_tables(routes, route_weights, experts_total)
+    base = stream + shared_result
+    return routed_layer(normed, tables, base, expert_gate[0], expert_up[0], expert_down[0])
 
 
 def solution(mesh):

time: 202 us -> 148 us (0.73)
  Pallas kernels: 0 us -> 111 us
  blocking collectives: 61.4 us -> 0 us
  waiting for transfers between devices: 54.6 us -> 6.68 us
  local copies, waits for them, and re-layouts: 32.5 us -> 4.22 us
  matrix products: 23.9 us -> 8.75 us
  other arithmetic: 13.3 us -> 5.99 us
  starting transfers between devices: 15.6 us -> 9.36 us
    pallas_call x0 -> x1, Pallas kernels: none -> 111 us  [routed_layer(): pl.pallas_call(moe_kernel, out_shape=jax.ShapeDtypeStruct((row_count, wid...]
    all_to_all x1 -> x0, blocking collectives: 61.4 us -> none  [body(): lax.all_to_all(outgoing, ('sp', 'tp'), split_axis=0, concat_axis=0, tiled...]
    all_to_all x1 -> x0, waiting for transfers between devices: 50.6 us -> none  [body(): lax.all_to_all(result.reshape(leading + (model_width,)), ('sp', 'tp'), sp...]
    gather x2 -> x0, local copies, waits for them, and re-layouts: 15.8 us -> none  [the longest x1 9.82 us: body(): flat_returned[slot_index].reshape(row_count, top_count, model_width)]
    dot_general x1 -> x2, matrix products: 9.96 us -> 0.57 us  [the longest x1 0.38 us: slot_tables(): spread = jnp.dot(stacked, expand, preferred_element_type=jnp.float32)]
    convert_element_type x1 -> x0, local copies, waits for them, and re-layouts: 6.55 us -> none  [body(): flat_returned[slot_index].reshape(row_count, top_count, model_width)]
    reduce_sum x3, other arithmetic: 8.01 us -> 1.87 us  [the longest x1 0.97 us: slot_tables(): mask = jnp.sum(named.astype(jnp.float32), axis=1)]
    all_to_all x1 -> x0, starting transfers between devices: 5.61 us -> none  [body(): lax.all_to_all(result.reshape(leading + (model_width,)), ('sp', 'tp'), sp...]
  transfers between devices with their start and end apart: 3 -> 2, of which waited for: 2 -> 1; matrix products, arithmetic and copies ran while one was open for 5% -> 3% of each run, Pallas kernels for 0% -> 0%
where the time goes in v2:
time: 148 us; the launch traced here: 146 us
  Pallas kernels  111 us (75%)
  starting transfers between devices  9.36 us (6%)
  matrix products  8.75 us (6%)
  waiting for transfers between devices  6.68 us (5%)
  other arithmetic  5.99 us (4%)
  local copies, waits for them, and re-layouts  4.22 us (3%)
    pallas_call x1, Pallas kernels, routed_layer(): pl.pallas_call(moe_kernel, out_shape=jax.ShapeDtypeStruct((row_count, wid...  111 us
    all_to_all x1, waiting for transfers between devices, body(): lax.all_to_all(conv_out, 'tp', split_axis=0, concat_axis=1, tiled=True)  6.68 us
    all_to_all x1, starting transfers between devices, body(): lax.all_to_all(conv_out, 'tp', split_axis=0, concat_axis=1, tiled=True)  5.42 us
    dot_general x1, matrix products, project_norm(): jnp.dot(scaled, out_proj, preferred_element_type=jnp.float32)  4.13 us
    ppermute x1, starting transfers between devices, from_behind(): return lax.ppermute(block, axis, route)  3.94 us
    dot_general x1, matrix products, body(): jnp.dot(swiglu_hidden(normed, shared_gate, shared_up), shared_down, prefe...  3.59 us
  transfers between devices with their start and end apart: 2, of which 1 were waited for; matrix products, arithmetic and copies ran while one was open for 3% of the time, Pallas kernels for 0%

profile of v2, /device:TPU:1, one launch (start us, length us, event | category | flops | bytes accessed | tf_op | source)
XLA Modules:
  0.0 145.7 jit_solution(9603882110750976738)
XLA Ops:
  0.0 0.0 copy-start
  0.0 0.0 copy-start.6
  0.0 0.0 copy-start.3
  0.0 1.4 convert_multiply_fusion
  1.4 0.1 slice.24
  1.5 3.9 %collective-permute-start = (f32[2,192]{0,1:T(8,128)S(1)}, f32[2,192]{0,1:T(8,128)S(1)}, u32[]{:S(2)}, u32[]{:S(2)}) collective-permute-start(f32[2,192]{0,1:T(8,128)S(1)} %slice.24), channel_id=1, source_target_pairs={{0,8},{8,16},{16,24},{24,32},{32,40},{40,48},{48,56},{56,64},{64,7... | collective-permute-start | bytes 4616 | tf_op jit(solution)/shard_map/ppermute | solution.py:304
  5.5 0.8 fusion.40
  6.3 0.7 reduce_sum.76
  7.0 0.7 divide_multiply_fusion
  7.7 0.0 copy-start.4
  7.7 1.0 convert_reduce_fusion
  8.7 0.2 fusion.22
  8.9 0.2 select_reduce_fusion.1
  9.1 0.0 collective-permute-done
  9.1 0.0 copy-done.3
  9.1 1.3 copy_bitcast_fusion
  10.4 5.4 %all-to-all-start = ((bf16[8,128,192]{1,2,0:T(8,128)(2,1)}), bf16[8,128,192]{1,2,0:T(8,128)(2,1)S(1)}, u32[]{:S(2)}, u32[]{:S(2)}) async-start(bf16[8,128,192]{1,2,0:T(8,128)(2,1)} %copy_bitcast_fusion), calls=%async_computation | async-start | bytes 786432 | tf_op jit(solution)/shard_map/all_to_all | solution.py:348
  15.9 0.0 copy-done.6
  15.9 0.4 fusion.3
  16.3 0.6 pad.4.tables
  16.9 6.7 %all-to-all-done = bf16[8,128,192]{1,2,0:T(8,128)(2,1)S(1)} async-done(((bf16[8,128,192]{1,2,0:T(8,128)(2,1)}), bf16[8,128,192]{1,2,0:T(8,128)(2,1)S(1)}, u32[]{:S(2)}, u32[]{:S(2)}) %all-to-all-start) | async-done | bytes 393248 | tf_op jit(solution)/shard_map/all_to_all | solution.py:348
  23.6 0.2 multiply_reduce_fusion.1
  23.8 0.0 copy-done.4
  23.8 0.3 fusion.11
  24.1 0.0 copy-start.5
  24.1 0.0 copy-start.2
  24.1 4.1 %multiply_reduce_fusion = (f32[128]{0:T(128)S(1)}, f32[128,2048]{1,0:T(8,128)S(1)}) fusion(f32[128]{0:T(128)S(1)} %add_rsqrt_fusion.1, bf16[128,1536]{0,1:T(8,128)(2,1)S(1)} %fusion.11, bf16[1536,2048]{1,0:T(8,128)(2,1)} %param.22, bf16[128,2048]{1,0:T(8,128)(2,1)} %param.23), kind=kOutput, calls=%fused_computation.10 | convolution fusion | flops 806616960 | bytes 8258560 | tf_op jit(solution)/shard_map/dot_general | solution.py:311
  28.2 0.0 copy-done.5
  28.3 0.2 multiply_convert_fusion.normed
  28.4 0.0 copy-start.1
  28.4 0.8 copy-done.1
  29.2 0.0 copy-done.2
  29.2 0.4 fusion.41
  29.7 0.0 copy-done
  29.7 3.6 %convolution_add_fusion.base = f32[128,2048]{1,0:T(8,128)} fusion(f32[128,2048]{1,0:T(8,128)S(1)} %get-tuple-element.15, bf16[512,2048]{1,0:T(8,128)(2,1)S(1)} %copy-done, bf16[128,2048]{1,0:T(8,128)(2,1)} %copy-done.1, bf16[2048,512]{1,0:T(8,128)(2,1)} %param.28, f32[128,512]{1,0:T(8,128)S(1)} %fusion.41), kind=kOutput, calls=%fused_computation.3 | convolution fusion | flops 537526272 | bytes 7077888 | tf_op jit(solution)/shard_map/dot_general | solution.py:353
  33.3 110.5 %routed_layer.1 = bf16[128,2048]{1,0:T(8,128)(2,1)} custom-call(bf16[128,2048]{1,0:T(8,128)(2,1)} %copy-done.1, f32[3,4,8,256]{3,2,1,0:T(8,128)} %pad.4.tables, f32[128,2048]{1,0:T(8,128)} %convolution_add_fusion.base, bf16[2048,512]{1,0:T(8,128)(2,1)} %bitcast.33, bf16[2048,512]{1,0:T(8,128)(2,1)} %bitcast.34, bf16[512,2048]{1,0:T(8,128)(2,1)} %bitcast.35), custom_call_target="tpu_custom_call" | custom-call | tf_op jit(solution)/shard_map/routed_layer/pallas_call | solution.py:288
  143.8 1.9 %copy.32 = bf16[128,2048]{1,0:T(8,128)(2,1)} copy(bf16[128,2048]{1,0:T(8,128)(2,1)} %routed_layer.1) | data formatting | bytes 1048576
  (8 shorter events, 0.1 us)
Async XLA Ops:
  0.0 29.7 %copy-start = (bf16[512,2048]{1,0:T(8,128)(2,1)S(1)}, bf16[512,2048]{1,0:T(8,128)(2,1)}, u32[]{:S(2)}) copy-start(bf16[512,2048]{1,0:T(8,128)(2,1)} %param.29) | copy-start | bytes 6291460
  0.0 15.9 %copy-start.6 = (s32[3072]{0:T(1024)S(1)}, s32[3072]{0:T(1024)}, u32[]{:S(2)}) copy-start(s32[3072]{0:T(1024)} %constant.46.clone) | copy-start | bytes 36868
  0.0 9.1 %copy-start.3 = (bf16[1024,192]{0,1:T(8,128)(2,1)S(1)}, bf16[1024,192]{0,1:T(8,128)(2,1)}, u32[]{:S(2)}) copy-start(bf16[1024,192]{0,1:T(8,128)(2,1)} %param.17) | copy-start | bytes 1179652
  1.5 7.6 %collective-permute-start = (f32[2,192]{0,1:T(8,128)S(1)}, f32[2,192]{0,1:T(8,128)S(1)}, u32[]{:S(2)}, u32[]{:S(2)}) collective-permute-start(f32[2,192]{0,1:T(8,128)S(1)} %slice.24), channel_id=1, source_target_pairs={{0,8},{8,16},{16,24},{24,32},{32,40},{40,48},{48,56},{56,64},{64,7... | collective-permute-start | bytes 4616 | tf_op jit(solution)/shard_map/ppermute | solution.py:304
  7.7 16.1 %copy-start.4 = (f32[1536]{0:T(1024)S(1)}, f32[1536]{0:T(1024)}, u32[]{:S(2)}) copy-start(f32[1536]{0:T(1024)} %param.21) | copy-start | bytes 18436
  10.4 13.1 %all-to-all-start = ((bf16[8,128,192]{1,2,0:T(8,128)(2,1)}), bf16[8,128,192]{1,2,0:T(8,128)(2,1)S(1)}, u32[]{:S(2)}, u32[]{:S(2)}) async-start(bf16[8,128,192]{1,2,0:T(8,128)(2,1)} %copy_bitcast_fusion), calls=%async_computation | async-start | bytes 786432 | tf_op jit(solution)/shard_map/all_to_all | solution.py:348
  24.1 4.2 %copy-start.5 = (f32[2048]{0:T(1024)S(1)}, f32[2048]{0:T(1024)}, u32[]{:S(2)}) copy-start(f32[2048]{0:T(1024)} %param.24) | copy-start | bytes 24580
  24.1 5.1 %copy-start.2 = (bf16[2048,512]{1,0:T(8,128)(2,1)S(1)}, bf16[2048,512]{1,0:T(8,128)(2,1)}, u32[]{:S(2)}) copy-start(bf16[2048,512]{1,0:T(8,128)(2,1)} %param.27) | copy-start | bytes 6291460
  28.4 0.8 copy-start.1

commit v3 on v0

v3 whole, which is shorter than its diff:
```python
import jax
import jax.numpy as jnp
from jax import lax
from jax.experimental import pallas as pl
from jax.experimental.pallas import tpu as pltpu
from jax.sharding import PartitionSpec as P

AXES = ("z", "x", "y")
ORDERS = (("z", "x", "y"), ("x", "y", "z"), ("y", "z", "x"))
CHUNKS = ((384, 384, 384), (256, 256, 384))
RING = 4
CORES = 2
SLOTS = 8
MESH = pl.DeviceIdType.MESH
PAIRS = tuple((g, h) for g in (1, 3, 2, 0) for h in range(CORES) if (g, h) != (0, 0))
NEAR_FIRST = (1, 3, 2)
EPS = 1e-06


def make_lanes():
    lanes, start = [], 0
    for chunk in CHUNKS:
        for color, width in enumerate(chunk):
            lanes.append((color, start, width))
            start += width
    return tuple(lanes)


LANES = make_lanes()
COLORS = len(ORDERS)


def layer_kernel(
    h_out_gate, h_in_gate, h_values, taps, mix_gain, h_proj, h_residual, ffn_gain,
    routes, route_weights, h_sgate, h_sup, h_sdown, h_gate, h_up, h_down,
    out,
    v_out_gate, v_in_gate, v_values, v_proj, v_residual, v_sgate, v_sup, v_sdown,
    v_gate, v_up, v_down,
    mixed, halo, conv, token_rows, base, normed, tables, seen_tab,
    arrived, result, acc_gate, acc_up, hidden, own_part, *rest,
):
    lanes = len(LANES)
    ag, pick, mid, slots, part, got = (rest[n * lanes : (n + 1) * lanes] for n in range(6))
    back = pick
    (load_s, halo_s, halo_r, mix_s, mix_r, tab_s, tab_r, ag_s, ag_r, p2_s, p2_r, p3_s, p3_r,
     r1_s, r1_r, r2_s, r2_r, r3_s, r3_r) = rest[6 * lanes :]
    sp, tp = lax.axis_index("sp"), lax.axis_index("tp")
    sp_count = RING * RING
    at = {"z": sp // RING, "x": sp % RING, "y": tp // CORES}
    core = tp % CORES
    bf16, f32 = jnp.bfloat16, jnp.float32

    def device(core_step=0, **steps):
        p = {k: (at[k] + steps.get(k, 0) + RING) % RING for k in AXES}
        return (p["z"] * RING + p["x"], p["y"] * CORES + (core + core_step + CORES) % CORES)

    def copy_to(src, dst, s, r, target):
        return pltpu.make_async_remote_copy(
            src_ref=src, dst_ref=dst, send_sem=s, recv_sem=r, device_id=target, device_id_type=MESH
        )

    def send(*args):
        copy = copy_to(*args)
        copy.start()
        return copy

    pairs_of_refs = (
        (h_in_gate, v_in_gate), (h_values, v_values), (h_out_gate, v_out_gate),
        (h_proj, v_proj), (h_residual, v_residual), (h_sgate, v_sgate), (h_sup, v_sup),
        (h_sdown, v_sdown), (h_gate, v_gate), (h_up, v_up), (h_down, v_down),
    )
    loads = [
        pltpu.make_async_copy(src, dst, load_s.at[n]) for n, (src, dst) in enumerate(pairs_of_refs)
    ]
    for load in loads:
        load.start()

    barrier = pltpu.get_barrier_semaphore()
    next_sp, last_sp = (sp + 1) % sp_count, (sp + sp_count - 1) % sp_count
    peers = [(next_sp, tp), (last_sp, tp), device(1)] + [
        device(h, **{axis: g}) for axis in AXES for g in range(1, RING) for h in range(CORES)
    ]
    for peer in peers:
        pl.semaphore_signal(barrier, inc=1, device_id=peer, device_id_type=MESH)

    row_count = normed.shape[0]
    channels, length = v_values.shape
    blocks = length // row_count
    for load in loads[0:2]:
        load.wait()
    mixed[:, row_count:] = v_in_gate[...].astype(f32) * v_values[...].astype(f32)
    pl.semaphore_wait(barrier, len(peers))
    halo_copy = send(mixed.at[:, pl.ds(length, row_count)], halo, halo_s, halo_r, (next_sp, tp))
    loads[2].wait()

    tap_columns = []
    for n in range(taps.shape[0]):
        wide = jnp.concatenate(
            [taps[n : n + 1, :], jnp.zeros((1, 2 * row_count - channels), f32)], axis=1
        )
        wide = jnp.broadcast_to(wide, (row_count, 2 * row_count))
        tap_columns.append(jnp.transpose(wide)[0:channels, :])

    def filter_block(j):
        window = mixed[:, j * row_count : (j + 2) * row_count]
        some = tap_columns[0] * pltpu.roll(window, 2, 1)[:, row_count:]
        some = some + tap_columns[1] * pltpu.roll(window, 1, 1)[:, row_count:]
        some = some + tap_columns[2] * window[:, row_count:]
        gate = v_out_gate[:, j * row_count : (j + 1) * row_count].astype(f32)
        conv[j] = (gate * some).astype(bf16)

    for j in range(1, blocks):
        filter_block(j)
    mix_copy = []
    for n, (g, h) in enumerate(PAIRS):
        target = device(h, y=g)
        mix_copy.append(
            copy_to(conv.at[target[1]], token_rows.at[tp], mix_s.at[n], mix_r.at[n], target)
        )

        @pl.when(target[1] != 0)
        def _(copy=mix_copy[n]):
            copy.start()

    experts_total = RING * RING * RING * CORES
    lane = lax.broadcasted_iota(jnp.int32, (row_count, experts_total), 1)
    down_row = lax.broadcasted_iota(jnp.int32, (row_count, experts_total), 0)
    weights = route_weights[...]
    gate_values = weights / jnp.sum(weights, axis=0, keepdims=True) * 2.5
    mask = jnp.zeros((experts_total, row_count), f32)
    gates = jnp.zeros((experts_total, row_count), f32)
    for k in range(routes.shape[0]):
        named = routes[k : k + 1, :] == down_row
        mask = jnp.where(named, 1.0, mask)
        gates = jnp.where(named, gate_values[k : k + 1, :], gates)
    mask, gates = jnp.transpose(mask), jnp.transpose(gates)
    earlier = jnp.where(lane < down_row, 1.0, 0.0).astype(bf16)
    rank = jnp.dot(earlier, mask.astype(bf16), preferred_element_type=f32)
    rank = jnp.where(mask > 0, rank, -1.0)
    numbers_here = (down_row + 1).astype(f32)
    token_list, gate_list = [], []
    for r in range(SLOTS):
        chosen = rank == float(r)
        token_list.append(jnp.sum(jnp.where(chosen, numbers_here, 0.0), axis=0, keepdims=True))
        gate_list.append(jnp.sum(jnp.where(chosen, gates, 0.0), axis=0, keepdims=True))
    token = jnp.concatenate(token_list, axis=0)
    gate = jnp.concatenate(gate_list, axis=0)
    gate_high = gate.astype(bf16)
    gate_low = (gate - gate_high.astype(f32)).astype(bf16)
    listed = (token.astype(bf16), gate_high, gate_low)
    group = RING * CORES * SLOTS
    plane = RING * group
    slot = lax.broadcasted_iota(jnp.int32, (1, RING * plane), 1)
    expert = lax.broadcasted_iota(jnp.int32, (experts_total, RING * plane), 0)
    keep = (
        lax.broadcasted_iota(jnp.int32, (SLOTS, RING * plane), 1) & (SLOTS - 1)
    ) == lax.broadcasted_iota(jnp.int32, (SLOTS, RING * plane), 0)
    for color, (first, second, third) in enumerate(ORDERS):
        digit = {
            first: (slot >> 8) & (RING - 1),
            second: (slot >> 6) & (RING - 1),
            third: (slot >> 4) & (RING - 1),
        }
        expert_of = (digit["z"] << 5) + (digit["x"] << 3) + (digit["y"] << 1)
        expert_of = expert_of + ((slot >> 3) & (CORES - 1))
        spread = jnp.where(expert_of == expert, 1.0, 0.0).astype(bf16)
        for kind, values in enumerate(listed):
            wide = jnp.dot(values, spread, preferred_element_type=f32)
            row = jnp.sum(jnp.where(keep, wide, 0.0), axis=0, keepdims=True)
            for a in range(RING):
                tables[color, a, kind : kind + 1, :] = row[:, a * plane : (a + 1) * plane]
    sent = [halo_copy]
    tab_copy = {}

    def send_tables():
        for d in NEAR_FIRST:
            for color, (first, _, _) in enumerate(ORDERS):
                tab_copy[color, d] = send(
                    tables.at[color, (at[first] + d) % RING], seen_tab.at[color, d - 1],
                    tab_s.at[color, d - 1], tab_r.at[color, d - 1], device(**{first: d}),
                )
                sent.append(tab_copy[color, d])

    halo_copy.wait_recv()
    mixed[:, 0:row_count] = jnp.where(sp == 0, jnp.zeros_like(halo), halo[...])
    filter_block(0)
    for n, (g, h) in enumerate(PAIRS):
        target = device(h, y=g)

        @pl.when(target[1] == 0)
        def _(copy=mix_copy[n]):
            copy.start()

    send_tables()

    loads[3].wait()
    total_channels = blocks * channels

    pair = CORES * channels
    token_rows[tp] = conv[tp]
    squares = jnp.zeros((row_count, 1), f32)
    for g in (0,) + NEAR_FIRST:
        for n in range(len(PAIRS)):
            if PAIRS[n][0] == g:
                mix_copy[n].wait_recv()
        source = (at["y"] - g + RING) % RING
        values = token_rows[pl.ds(source * CORES, CORES)].reshape(pair, row_count)
        values = jnp.transpose(values.astype(f32))
        squares = squares + jnp.sum(values * values, axis=1, keepdims=True)
        step = pair // 128
        gain = jnp.concatenate([mix_gain[pl.ds(source * step + n, 1), :] for n in range(step)], axis=1)
        product = jnp.dot(
            (values * gain).astype(bf16), v_proj[source], preferred_element_type=f32
        )
        if g == 0:
            base[...] = product
        else:
            base[...] += product
    loads[4].wait()
    inverse = lax.rsqrt(squares / total_channels + EPS)
    stream = v_residual[...].astype(f32) + base[...] * inverse
    base[...] = stream
    norm = lax.rsqrt(jnp.mean(stream * stream, axis=1, keepdims=True) + EPS)
    normed[...] = (stream * norm * ffn_gain[...]).astype(bf16)

    def lead(color, i, d):
        return (d, i) if color == 2 else (i, d)

    def piece(ref, lane_at, g, h):
        color, c0, w = LANES[lane_at]
        cols = pl.ds(c0, w)
        if color == 0:
            return ref.at[:, :, g, h, :, cols]
        if color == 1:
            return ref.at[g, :, :, h, :, cols]
        return ref.at[:, g, :, h, :, cols]

    ag_copy = {}
    for d in NEAR_FIRST:
        for q, (color, c0, w) in enumerate(LANES):
            ag_copy[q, d] = send(
                normed.at[:, pl.ds(c0, w)], ag[q].at[d - 1],
                ag_s.at[q, d - 1], ag_r.at[q, d - 1], device(**{ORDERS[color][0]: d}),
            )
            sent.append(ag_copy[q, d])

    numbers = (lax.broadcasted_iota(jnp.int32, (row_count, plane), 0) + 1).astype(f32)

    def table(color, i):
        return tables[color, at[ORDERS[color][0]]] if i == 0 else seen_tab[color, i - 1]

    p2_copy = {}

    def pick_rows(q, i):
        color, c0, w = LANES[q]
        second = ORDERS[color][1]
        if i == 0:
            rows = normed[:, c0 : c0 + w]
        else:
            ag_copy[q, i].wait_recv()
            rows = ag[q][i - 1]
        onehot = jnp.where(numbers == table(color, i)[0:1, :], 1.0, 0.0).astype(bf16)
        picked = lax.dot_general(
            onehot, rows, (((0,), (0,)), ((), ())), preferred_element_type=f32
        )
        picked = picked.astype(bf16).reshape(RING, RING * CORES, SLOTS, w)
        for b in range(RING):
            pick[q][b, i] = picked[b]
        for d in NEAR_FIRST:
            p2_copy[q, d, i] = send(
                pick[q].at[(at[second] + d) % RING, i], mid[q].at[lead(color, i, d)],
                p2_s.at[q, d - 1, i], p2_r.at[q, d - 1, i], device(**{second: d}),
            )
        mid[q][lead(color, i, 0)] = pick[q][at[second], i]

    def swish(gate_part, up_part):
        return (gate_part / (1.0 + jnp.exp(-gate_part)) * up_part).astype(bf16)

    for q in range(lanes):
        pick_rows(q, 0)
    for load in loads[5:8]:
        load.wait()
    rows = normed[...]
    shared = swish(
        jnp.dot(rows, v_sgate[...], preferred_element_type=f32),
        jnp.dot(rows, v_sup[...], preferred_element_type=f32),
    )
    base[...] += jnp.dot(shared, v_sdown[...], preferred_element_type=f32)
    for i in NEAR_FIRST:
        for color in range(COLORS):
            tab_copy[color, i].wait_recv()
        for q in range(lanes):
            pick_rows(q, i)

    p3_copy = {}
    for q, (color, c0, w) in enumerate(LANES):
        third = ORDERS[color][2]
        for i in (0,) + NEAR_FIRST:
            for d in NEAR_FIRST:
                p2_copy[q, d, i].wait()
        for n, (g, h) in enumerate(PAIRS):
            k = (at[third] + g) % RING * CORES + (core + h) % CORES
            p3_copy[q, n] = send(
                mid[q].at[:, :, k], piece(arrived, q, g, h),
                p3_s.at[q, n], p3_r.at[q, n], device(h, **{third: g}),
            )
            sent.append(p3_copy[q, n])
        piece(arrived, q, 0, 0)[...] = mid[q][:, :, at[third] * CORES + core]

    for load in loads[8:]:
        load.wait()
    width = arrived.shape[-1]
    block = RING * RING * CORES * SLOTS
    split = sum(CHUNKS[0])
    half = lanes // 2
    for q in range(half):
        for n in range(len(PAIRS)):
            p3_copy[q, n].wait_recv()

    @pl.loop(0, RING)
    def _(zi):
        rows = arrived[zi, :, :, :, :, 0:split].reshape(block, split)
        acc_gate[zi] = jnp.dot(rows, v_gate[0:split, :], preferred_element_type=f32)
        acc_up[zi] = jnp.dot(rows, v_up[0:split, :], preferred_element_type=f32)

    for q in range(half, lanes):
        for n in range(len(PAIRS)):
            p3_copy[q, n].wait_recv()

    @pl.loop(0, RING)
    def _(zi):
        rows = arrived[zi, :, :, :, :, split:width].reshape(block, width - split)
        gate_part = acc_gate[zi] + jnp.dot(rows, v_gate[split:width, :], preferred_element_type=f32)
        up_part = acc_up[zi] + jnp.dot(rows, v_up[split:width, :], preferred_element_type=f32)
        hidden[zi] = swish(gate_part, up_part)

    r1_copy = {}
    for start, stop, chunk in ((0, split, range(half)), (split, width, range(half, lanes))):

        @pl.loop(0, RING)
        def _(zi):
            done = jnp.dot(hidden[zi], v_down[:, start:stop], preferred_element_type=f32)
            result[zi, :, :, :, :, start:stop] = done.astype(bf16).reshape(
                RING, RING, CORES, SLOTS, stop - start
            )

        for n, (g, h) in enumerate(PAIRS):
            for q in chunk:
                third = ORDERS[LANES[q][0]][2]
                r1_copy[q, n] = send(
                    piece(result, q, g, h), back[q].at[:, :, at[third] * CORES + core],
                    r1_s.at[q, n], r1_r.at[q, n], device(-h, **{third: -g}),
                )
                sent.append(r1_copy[q, n])

    r2_copy = {}
    for q, (color, c0, w) in enumerate(LANES):
        _, second, third = ORDERS[color]
        back[q][:, :, at[third] * CORES + core] = piece(result, q, 0, 0)[...]
        for n in range(len(PAIRS)):
            r1_copy[q, n].wait_recv()
        for d in NEAR_FIRST:
            src = back[q].at[d] if color == 2 else back[q].at[:, d]
            r2_copy[q, d] = send(
                src, slots[q].at[:, at[second]],
                r2_s.at[q, d - 1], r2_r.at[q, d - 1], device(**{second: -d}),
            )
            sent.append(r2_copy[q, d])
        slots[q][:, at[second]] = back[q][0] if color == 2 else back[q][:, 0]
    r3_copy = {}
    for q, (color, c0, w) in enumerate(LANES):
        first = ORDERS[color][0]
        for d in NEAR_FIRST:
            r2_copy[q, d].wait_recv()
        for i in NEAR_FIRST + (0,):
            rows = slots[q][i].reshape(plane, w)
            tab = table(color, i)
            hit = numbers == tab[0:1, :]
            high = jnp.where(hit, tab[1:2, :], 0.0).astype(bf16)
            low = jnp.where(hit, tab[2:3, :], 0.0).astype(bf16)
            some = jnp.dot(high, rows, preferred_element_type=f32) + jnp.dot(
                low, rows, preferred_element_type=f32
            )
            if i == 0:
                own_part[:, c0 : c0 + w] = some
            else:
                part[q][i - 1] = some.astype(bf16)
                r3_copy[q, i] = send(
                    part[q].at[i - 1], got[q].at[i - 1],
                    r3_s.at[q, i - 1], r3_r.at[q, i - 1], device(**{first: -i}),
                )
                sent.append(r3_copy[q, i])
    for q, (_, c0, w) in enumerate(LANES):
        some = own_part[:, c0 : c0 + w] + base[:, c0 : c0 + w]
        for i in NEAR_FIRST:
            r3_copy[q, i].wait_recv()
            some = some + got[q][i - 1].astype(f32)
        out[:, c0 : c0 + w] = some.astype(bf16)
    for copy in sent:
        copy.wait_send()
    for copy in mix_copy:
        copy.wait_send()


def body(
    out_gate, in_gate, conv_values, conv_taps, mix_gain, out_proj, residual, ffn_gain,
    routes, route_weights, shared_gate, shared_up, shared_down,
    expert_gate, expert_up, expert_down,
):
    length, channels = conv_values.shape
    row_count, width = residual.shape
    blocks = length // row_count
    unit = expert_gate.shape[2]
    shared_unit = shared_gate.shape[1]
    bf16, f32 = jnp.bfloat16, jnp.float32
    lanes = len(LANES)
    widths = [w for _, _, w in LANES]

    def per_lane(*shape):
        return [pltpu.VMEM(shape + (w,), bf16) for w in widths]

    def vmem(*shape, dtype=bf16):
        return pltpu.VMEM(shape, dtype)

    dma = pltpu.SemaphoreType.DMA
    near, pairs = RING - 1, len(PAIRS)
    plane = RING * RING * CORES * SLOTS
    scratch = (
        [vmem(channels, length)] * 3
        + [vmem(RING, CORES * channels, width), vmem(row_count, width)]
        + [vmem(width, shared_unit), vmem(width, shared_unit), vmem(shared_unit, width)]
        + [vmem(width, unit), vmem(width, unit), vmem(unit, width)]
        + [vmem(channels, row_count + length, dtype=f32), vmem(channels, row_count, dtype=f32)]
        + [vmem(blocks, channels, row_count)] * 2
        + [vmem(row_count, width, dtype=f32), vmem(row_count, width)]
        + [vmem(COLORS, RING, 8, plane, dtype=f32), vmem(COLORS, near, 8, plane, dtype=f32)]
        + [vmem(RING, RING, RING, CORES, SLOTS, width)] * 2
        + [vmem(RING, plane, unit, dtype=f32)] * 2
        + [vmem(RING, plane, unit), vmem(row_count, width, dtype=f32)]
        + per_lane(near, row_count)
        + per_lane(RING, RING, RING * CORES, SLOTS)
        + per_lane(RING, RING, RING * CORES, SLOTS)
        + per_lane(RING, RING, RING * CORES, SLOTS)
        + per_lane(near, row_count)
        + per_lane(near, row_count)
        + [dma((11,)), dma, dma, dma((pairs,)), dma((pairs,))]
        + [dma((COLORS, near))] * 2
        + [dma((lanes, near))] * 2
        + [dma((lanes, near, RING))] * 2
        + [dma((lanes, pairs))] * 4
        + [dma((lanes, near))] * 4
    )
    whole = pl.BlockSpec(memory_space=pltpu.VMEM)
    hbm = pl.BlockSpec(memory_space=pl.ANY)
    return pl.pallas_call(
        layer_kernel,
        out_shape=jax.ShapeDtypeStruct((row_count, width), bf16),
        in_specs=[hbm, hbm, hbm, whole, whole, hbm, hbm, whole, whole, whole] + [hbm] * 6,
        out_specs=whole,
        scratch_shapes=scratch,
        compiler_params=pltpu.CompilerParams(
            collective_id=0, has_side_effects=True, vmem_limit_bytes=67043328
        ),
        name="whole_layer",
    )(
        out_gate.T, in_gate.T, conv_values.T, conv_taps, mix_gain.reshape(-1, 128),
        out_proj.reshape(RING, CORES * channels, width), residual, ffn_gain.reshape(1, width),
        routes.T, route_weights.T, shared_gate, shared_up, shared_down,
        expert_gate[0], expert_up[0], expert_down[0],
    )


def solution(mesh):
    in_specs = (
        P("sp", "tp"),
        P("sp", "tp"),
        P("sp", "tp"),
        P(None, "tp"),
        P(),
        P(),
        P(("sp", "tp"), None),
        P(),
        P(("sp", "tp"), None),
        P(("sp", "tp"), None),
        P(),
        P(),
        P(),
        P(("sp", "tp"), None, None),
        P(("sp", "tp"), None, None),
        P(("sp", "tp"), None, None),
    )
    out_specs = P(("sp", "tp"), None)
    return jax.shard_map(body, mesh=mesh, in_specs=in_specs, out_specs=out_specs, check_vma=False)
```

time: 202 us -> 115 us (0.57)
  Pallas kernels: 0 us -> 113 us
  blocking collectives: 61.4 us -> 0 us
  waiting for transfers between devices: 54.6 us -> 0 us
  local copies, waits for them, and re-layouts: 32.5 us -> 1.88 us
  matrix products: 23.9 us -> 0 us
  starting transfers between devices: 15.6 us -> 0 us
  other arithmetic: 13.3 us -> 0 us
    pallas_call x0 -> x1, Pallas kernels: none -> 113 us  [body(): pl.pallas_call(layer_kernel, out_shape=jax.ShapeDtypeStruct((row_count, w...]
    all_to_all x1 -> x0, blocking collectives: 61.4 us -> none  [body(): lax.all_to_all(outgoing, ('sp', 'tp'), split_axis=0, concat_axis=0, tiled...]
    all_to_all x2 -> x0, waiting for transfers between devices: 54.6 us -> none  [the longest x1 50.6 us: body(): lax.all_to_all(result.reshape(leading + (model_width,)), ('sp', 'tp'), sp...]
    dot_general x5 -> x0, matrix products: 23.9 us -> none  [the longest x1 9.96 us: body(): jnp.dot(hidden, expert_down[0], preferred_element_type=jnp.float32)]
    gather x2 -> x0, local copies, waits for them, and re-layouts: 15.8 us -> none  [the longest x1 9.82 us: body(): flat_returned[slot_index].reshape(row_count, top_count, model_width)]
    all_to_all x2 -> x0, starting transfers between devices: 11 us -> none  [the longest x1 5.61 us: body(): lax.all_to_all(result.reshape(leading + (model_width,)), ('sp', 'tp'), sp...]
    reduce_sum x4 -> x0, other arithmetic: 8.23 us -> none  [the longest x1 7.69 us: body(): routed = jnp.sum(picked * gate_values[:, :, None], axis=1)]
    convert_element_type x1 -> x0, local copies, waits for them, and re-layouts: 6.55 us -> none  [body(): flat_returned[slot_index].reshape(row_count, top_count, model_width)]
  transfers between devices with their start and end apart: 3 -> 0, of which waited for: 2 -> 0; matrix products, arithmetic and copies ran while one was open for 5% -> 0% of each run, Pallas kernels for 0% -> 0%
where the time goes in v3:
time: 115 us
  Pallas kernels  113 us (98%)
  local copies, waits for them, and re-layouts  1.88 us (2%)
    pallas_call x1, Pallas kernels, body(): pl.pallas_call(layer_kernel, out_shape=jax.ShapeDtypeStruct((row_count, w...  113 us

profile of v3, /device:TPU:1, one launch (start us, length us, event | category | flops | bytes accessed | tf_op | source)
XLA Modules:
  0.0 114.7 jit_solution(204089079278123120)
XLA Ops:
  0.0 112.8 %whole_layer.1 = bf16[128,2048]{1,0:T(8,128)(2,1)} custom-call(bf16[192,1024]{1,0:T(8,128)(2,1)} %bitcast.15, bf16[192,1024]{1,0:T(8,128)(2,1)} %bitcast.16, bf16[192,1024]{1,0:T(8,128)(2,1)} %bitcast.17, f32[3,192]{1,0:T(4,128)} %taps.1, f32[12,128]{1,0:T(8,128)} %bitcast.18, bf16[4,384,2048]{2,1,0:T(8,128)(2,1)} %bitcast.11, bf16[128,2048]{1,0:T(8,128)(2,1)} %h_residual.1, ...), custom_call_target="tpu_custom_call" | custom-call | tf_op jit(solution)/shard_map/whole_layer/pallas_call | solution.py:455
  112.8 1.9 %copy.18 = bf16[128,2048]{1,0:T(8,128)(2,1)} copy(bf16[128,2048]{1,0:T(8,128)(2,1)} %whole_layer.1) | data formatting | bytes 1048576

commit v4 on v3

v4 whole, which is shorter than its diff:
```python
import jax
import jax.numpy as jnp
from jax import lax
from jax.experimental import pallas as pl
from jax.experimental.pallas import tpu as pltpu
from jax.sharding import PartitionSpec as P

AXES = ("z", "x", "y")
ORDERS = (("z", "x", "y"), ("x", "y", "z"), ("y", "z", "x"))
CHUNKS = ((256, 256, 256), (256, 256, 256), (128, 128, 256))
RING = 4
CORES = 2
SLOTS = 8
MESH = pl.DeviceIdType.MESH
PAIRS = tuple((g, h) for g in (2, 1, 3, 0) for h in range(CORES) if (g, h) != (0, 0))
NEAR_FIRST = (1, 3, 2)
FAR_FIRST = (2, 1, 3)
EPS = 1e-06


def make_lanes():
    lanes, start = [], 0
    for chunk in CHUNKS:
        for color, width in enumerate(chunk):
            lanes.append((color, start, width))
            start += width
    return tuple(lanes)


LANES = make_lanes()
CHUNK_ENDS = tuple(sum(sum(c) for c in CHUNKS[: n + 1]) for n in range(len(CHUNKS)))
COLORS = len(ORDERS)


def layer_kernel(
    h_out_gate, h_in_gate, h_values, h_taps, h_mix_gain, h_proj, h_residual, h_ffn_gain,
    h_routes, h_route_weights, h_sgate, h_sup, h_sdown, h_gate, h_up, h_down,
    out,
    v_out, taps, mix_gain, ffn_gain, routes, route_weights,
    v_out_gate, v_in_gate, v_values, v_proj, v_residual, v_sgate, v_sup, v_sdown,
    v_gate, v_up, v_down,
    mixed, halo_out, halo, conv, token_rows, base, normed, tables, seen_tab,
    arrived, result, acc_gate, acc_up, hidden, own_part, *rest,
):
    lanes = len(LANES)
    ag, pick, mid, slots, part, got = (rest[n * lanes : (n + 1) * lanes] for n in range(6))
    back = pick
    (load_s, halo_s, halo_r, mix_s, mix_r, tab_s, tab_r, ag_s, ag_r, p2_s, p2_r, p3_s, p3_r,
     r1_s, r1_r, r2_s, r2_r, r3_s, r3_r, out_s) = rest[6 * lanes :]
    sp, tp = lax.axis_index("sp"), lax.axis_index("tp")
    sp_count = RING * RING
    at = {"z": sp // RING, "x": sp % RING, "y": tp // CORES}
    core = tp % CORES
    bf16, f32 = jnp.bfloat16, jnp.float32

    def device(core_step=0, **steps):
        p = {k: (at[k] + steps.get(k, 0) + RING) % RING for k in AXES}
        return (p["z"] * RING + p["x"], p["y"] * CORES + (core + core_step + CORES) % CORES)

    def copy_to(src, dst, s, r, target):
        return pltpu.make_async_remote_copy(
            src_ref=src, dst_ref=dst, send_sem=s, recv_sem=r, device_id=target, device_id_type=MESH
        )

    def send(*args):
        copy = copy_to(*args)
        copy.start()
        return copy

    pairs_of_refs = (
        (h_routes, routes), (h_route_weights, route_weights), (h_in_gate, v_in_gate),
        (h_values, v_values), (h_taps, taps), (h_out_gate, v_out_gate),
        (h_mix_gain, mix_gain), (h_proj, v_proj), (h_residual, v_residual),
        (h_ffn_gain, ffn_gain), (h_sgate, v_sgate), (h_sup, v_sup), (h_sdown, v_sdown),
        (h_gate, v_gate), (h_up, v_up), (h_down, v_down),
    )
    loads = [
        pltpu.make_async_copy(src, dst, load_s.at[n]) for n, (src, dst) in enumerate(pairs_of_refs)
    ]

    def drain(ref, semaphore):
        pltpu.make_async_copy(ref, ref, semaphore).wait()

    barrier = pltpu.get_barrier_semaphore()
    next_sp, last_sp = (sp + 1) % sp_count, (sp + sp_count - 1) % sp_count
    peers = [(next_sp, tp), (last_sp, tp), device(1)] + [
        device(h, **{axis: g}) for axis in AXES for g in range(1, RING) for h in range(CORES)
    ]
    for peer in peers:
        pl.semaphore_signal(barrier, inc=1, device_id=peer, device_id_type=MESH)

    for load in loads[0:6]:
        load.start()
    row_count = normed.shape[0]
    channels, length = v_values.shape
    blocks = length // row_count
    for load in loads[2:6]:
        load.wait()
    for load in loads[6:]:
        load.start()
    mixed[:, row_count:] = v_in_gate[...].astype(f32) * v_values[...].astype(f32)
    spare = 2 * row_count - channels
    tail = jnp.concatenate(
        [mixed[:, length : length + row_count], jnp.zeros((spare, row_count), f32)], axis=0
    )
    halo_out[...] = jnp.transpose(tail)[row_count - 8 :, :]
    tap_columns = []
    for n in range(taps.shape[0]):
        wide = jnp.concatenate(
            [taps[n : n + 1, :], jnp.zeros((1, 2 * row_count - channels), f32)], axis=1
        )
        wide = jnp.broadcast_to(wide, (row_count, 2 * row_count))
        tap_columns.append(jnp.transpose(wide)[0:channels, :])

    def filter_block(j):
        window = mixed[:, j * row_count : (j + 2) * row_count]
        some = tap_columns[0] * pltpu.roll(window, 2, 1)[:, row_count:]
        some = some + tap_columns[1] * pltpu.roll(window, 1, 1)[:, row_count:]
        some = some + tap_columns[2] * window[:, row_count:]
        gate = v_out_gate[:, j * row_count : (j + 1) * row_count].astype(f32)
        conv[j] = (gate * some).astype(bf16)

    for j in range(1, blocks):
        filter_block(j)
    pl.semaphore_wait(barrier, len(peers))
    halo_copy = send(halo_out, halo, halo_s, halo_r, (next_sp, tp))

    def mix_sends(zero):
        for g, h in PAIRS:
            target = device(h, y=g)
            copy = copy_to(conv.at[target[1]], token_rows.at[tp], mix_s, mix_r.at[g], target)

            @pl.when((target[1] == 0) == zero)
            def _(copy=copy):
                copy.start()

    mix_sends(False)
    halo_copy.wait()
    late = jnp.concatenate(
        [jnp.zeros((row_count - 8, 2 * row_count), f32), halo[...]], axis=0
    )
    late = jnp.transpose(late)[0:channels, :]
    mixed[:, 0:row_count] = jnp.where(sp == 0, jnp.zeros_like(late), late)
    filter_block(0)
    mix_sends(True)

    for load in loads[0:2]:
        load.wait()
    experts_total = RING * RING * RING * CORES
    lane = lax.broadcasted_iota(jnp.int32, (row_count, experts_total), 1)
    down_row = lax.broadcasted_iota(jnp.int32, (row_count, experts_total), 0)
    weights = route_weights[...]
    gate_values = weights / jnp.sum(weights, axis=0, keepdims=True) * 2.5
    mask = jnp.zeros((experts_total, row_count), f32)
    gates = jnp.zeros((experts_total, row_count), f32)
    for k in range(routes.shape[0]):
        named = routes[k : k + 1, :] == down_row
        mask = jnp.where(named, 1.0, mask)
        gates = jnp.where(named, gate_values[k : k + 1, :], gates)
    mask, gates = jnp.transpose(mask), jnp.transpose(gates)
    earlier = jnp.where(lane < down_row, 1.0, 0.0).astype(bf16)
    rank = jnp.dot(earlier, mask.astype(bf16), preferred_element_type=f32)
    rank = jnp.where(mask > 0, rank, -1.0)
    numbers_here = (down_row + 1).astype(f32)
    token_list, gate_list = [], []
    for r in range(SLOTS):
        chosen = rank == float(r)
        token_list.append(jnp.sum(jnp.where(chosen, numbers_here, 0.0), axis=0, keepdims=True))
        gate_list.append(jnp.sum(jnp.where(chosen, gates, 0.0), axis=0, keepdims=True))
    token = jnp.concatenate(token_list, axis=0)
    gate = jnp.concatenate(gate_list, axis=0)
    gate_high = gate.astype(bf16)
    gate_low = (gate - gate_high.astype(f32)).astype(bf16)
    listed = (token.astype(bf16), gate_high, gate_low)
    group = RING * CORES * SLOTS
    plane = RING * group
    slot = lax.broadcasted_iota(jnp.int32, (1, RING * plane), 1)
    expert = lax.broadcasted_iota(jnp.int32, (experts_total, RING * plane), 0)
    keep = (
        lax.broadcasted_iota(jnp.int32, (SLOTS, RING * plane), 1) & (SLOTS - 1)
    ) == lax.broadcasted_iota(jnp.int32, (SLOTS, RING * plane), 0)
    for color, (first, second, third) in enumerate(ORDERS):
        digit = {
            first: (slot >> 8) & (RING - 1),
            second: (slot >> 6) & (RING - 1),
            third: (slot >> 4) & (RING - 1),
        }
        expert_of = (digit["z"] << 5) + (digit["x"] << 3) + (digit["y"] << 1)
        expert_of = expert_of + ((slot >> 3) & (CORES - 1))
        spread = jnp.where(expert_of == expert, 1.0, 0.0).astype(bf16)
        for kind, values in enumerate(listed):
            wide = jnp.dot(values, spread, preferred_element_type=f32)
            row = jnp.sum(jnp.where(keep, wide, 0.0), axis=0, keepdims=True)
            for a in range(RING):
                tables[color, a, kind : kind + 1, :] = row[:, a * plane : (a + 1) * plane]
    for d in FAR_FIRST:
        for color, (first, _, _) in enumerate(ORDERS):
            send(
                tables.at[color, (at[first] + d) % RING], seen_tab.at[d - 1, color],
                tab_s, tab_r.at[d - 1], device(**{first: d}),
            )

    for load in loads[6:8]:
        load.wait()
    total_channels = blocks * channels

    pair = CORES * channels
    token_rows[tp] = conv[tp]
    squares = jnp.zeros((row_count, 1), f32)
    for g in (0,) + NEAR_FIRST:
        drain(token_rows.at[pl.ds(0, CORES if g else 1)], mix_r.at[g])
        source = (at["y"] - g + RING) % RING
        values = token_rows[pl.ds(source * CORES, CORES)].reshape(pair, row_count)
        values = jnp.transpose(values.astype(f32))
        squares = squares + jnp.sum(values * values, axis=1, keepdims=True)
        step = pair // 128
        gain = jnp.concatenate([mix_gain[pl.ds(source * step + n, 1), :] for n in range(step)], axis=1)
        product = jnp.dot(
            (values * gain).astype(bf16), v_proj[source], preferred_element_type=f32
        )
        if g == 0:
            base[...] = product
        else:
            base[...] += product
    for load in loads[8:10]:
        load.wait()
    inverse = lax.rsqrt(squares / total_channels + EPS)
    stream = v_residual[...].astype(f32) + base[...] * inverse
    base[...] = stream
    norm = lax.rsqrt(jnp.mean(stream * stream, axis=1, keepdims=True) + EPS)
    normed[...] = (stream * norm * ffn_gain[...]).astype(bf16)

    def lead(color, i, d):
        return (d, i) if color == 2 else (i, d)

    def piece(ref, lane_at, g, h):
        color, c0, w = LANES[lane_at]
        cols = pl.ds(c0, w)
        if color == 0:
            return ref.at[:, :, g, h, :, cols]
        if color == 1:
            return ref.at[g, :, :, h, :, cols]
        return ref.at[:, g, :, h, :, cols]

    def gather_send(q, d, src, s):
        color = LANES[q][0]
        step = 1 if d == 1 or (d == 2 and q % 2 == 0) else -1
        send(src, ag[q].at[d - 1], s, ag_r.at[q, d - 1], device(**{ORDERS[color][0]: step}))

    for d in (1, 3):
        for q, (_, c0, w) in enumerate(LANES):
            gather_send(q, d, normed.at[:, pl.ds(c0, w)], ag_s.at[d - 1])

    numbers = (lax.broadcasted_iota(jnp.int32, (row_count, plane), 0) + 1).astype(f32)

    def table(color, i):
        return tables[color, at[ORDERS[color][0]]] if i == 0 else seen_tab[i - 1, color]

    def pick_rows(q, i):
        color, c0, w = LANES[q]
        second = ORDERS[color][1]
        if i == 0:
            rows = normed[:, c0 : c0 + w]
        else:
            drain(ag[q].at[i - 1], ag_r.at[q, i - 1])
            if i == (3 if q % 2 else 1):
                gather_send(q, 2, ag[q].at[i - 1], ag_s.at[1])
            rows = ag[q][i - 1]
        onehot = jnp.where(numbers == table(color, i)[0:1, :], 1.0, 0.0).astype(bf16)
        picked = lax.dot_general(
            onehot, rows, (((0,), (0,)), ((), ())), preferred_element_type=f32
        )
        picked = picked.astype(bf16).reshape(RING, RING * CORES, SLOTS, w)
        for b in range(RING):
            pick[q][b, i] = picked[b]
        for d in FAR_FIRST:
            send(
                pick[q].at[(at[second] + d) % RING, i], mid[q].at[lead(color, i, d)],
                p2_s.at[q], p2_r.at[q], device(**{second: d}),
            )
        mid[q][lead(color, i, 0)] = pick[q][at[second], i]

    def swish(gate_part, up_part):
        return (gate_part / (1.0 + jnp.exp(-gate_part)) * up_part).astype(bf16)

    for q in range(lanes):
        pick_rows(q, 0)
    for load in loads[10:13]:
        load.wait()
    rows = normed[...]
    shared = swish(
        jnp.dot(rows, v_sgate[...], preferred_element_type=f32),
        jnp.dot(rows, v_sup[...], preferred_element_type=f32),
    )
    base[...] += jnp.dot(shared, v_sdown[...], preferred_element_type=f32)
    for i in NEAR_FIRST:
        drain(seen_tab.at[i - 1], tab_r.at[i - 1])
    for turn in ((1, 3), (3, 1), (2, 2)):
        for q in range(lanes):
            pick_rows(q, turn[q % 2])

    near, pairs = RING - 1, len(PAIRS)
    for q, (color, c0, w) in enumerate(LANES):
        third = ORDERS[color][2]
        drain(mid[q].at[pl.ds(0, near)], p2_r.at[q])
        drain(pick[q].at[pl.ds(0, near)], p2_s.at[q])
        for g, h in PAIRS:
            k = (at[third] + g) % RING * CORES + (core + h) % CORES
            send(
                mid[q].at[:, :, k], piece(arrived, q, g, h),
                p3_s.at[q], p3_r.at[q], device(h, **{third: g}),
            )
        piece(arrived, q, 0, 0)[...] = mid[q][:, :, at[third] * CORES + core]

    for load in loads[13:]:
        load.wait()
    width = arrived.shape[-1]
    block = RING * RING * CORES * SLOTS
    spans = tuple(zip((0,) + CHUNK_ENDS, CHUNK_ENDS))
    for chunk, (start, stop) in enumerate(spans):
        for q in range(chunk * COLORS, (chunk + 1) * COLORS):
            drain(mid[q].at[:, :, pl.ds(0, pairs)], p3_r.at[q])

        @pl.loop(0, RING)
        def _(zi):
            rows = arrived[zi, :, :, :, :, start:stop].reshape(block, stop - start)
            gate_part = jnp.dot(rows, v_gate[start:stop, :], preferred_element_type=f32)
            up_part = jnp.dot(rows, v_up[start:stop, :], preferred_element_type=f32)
            if chunk > 0:
                gate_part = gate_part + acc_gate[zi]
                up_part = up_part + acc_up[zi]
            if chunk + 1 == len(spans):
                hidden[zi] = swish(gate_part, up_part)
            else:
                acc_gate[zi] = gate_part
                acc_up[zi] = up_part

    for chunk, (start, stop) in enumerate(spans):

        @pl.loop(0, RING)
        def _(zi):
            done = jnp.dot(hidden[zi], v_down[:, start:stop], preferred_element_type=f32)
            result[zi, :, :, :, :, start:stop] = done.astype(bf16).reshape(
                RING, RING, CORES, SLOTS, stop - start
            )

        for color in range(COLORS):
            q = chunk * COLORS + color
            third = ORDERS[color][2]
            for g, h in PAIRS:
                send(
                    piece(result, q, g, h), back[q].at[:, :, at[third] * CORES + core],
                    r1_s.at[q], r1_r.at[q], device(-h, **{third: -g}),
                )

    for q, (color, c0, w) in enumerate(LANES):
        _, second, third = ORDERS[color]
        back[q][:, :, at[third] * CORES + core] = piece(result, q, 0, 0)[...]
        drain(back[q].at[:, :, pl.ds(0, pairs)], r1_r.at[q])
        for d in FAR_FIRST:
            src = back[q].at[d] if color == 2 else back[q].at[:, d]
            send(
                src, slots[q].at[:, at[second]], r2_s.at[q], r2_r.at[q], device(**{second: -d})
            )
        slots[q][:, at[second]] = back[q][0] if color == 2 else back[q][:, 0]
    for q, (color, c0, w) in enumerate(LANES):
        first = ORDERS[color][0]
        drain(slots[q].at[:, pl.ds(0, near)], r2_r.at[q])
        for i in FAR_FIRST + (0,):
            rows = slots[q][i].reshape(plane, w)
            tab = table(color, i)
            hit = numbers == tab[0:1, :]
            high = jnp.where(hit, tab[1:2, :], 0.0).astype(bf16)
            low = jnp.where(hit, tab[2:3, :], 0.0).astype(bf16)
            some = jnp.dot(high, rows, preferred_element_type=f32) + jnp.dot(
                low, rows, preferred_element_type=f32
            )
            if i == 0:
                own_part[:, c0 : c0 + w] = some
            else:
                part[q][i - 1] = some.astype(bf16)
                send(
                    part[q].at[i - 1], got[q].at[i - 1], r3_s.at[q], r3_r.at[q],
                    device(**{first: -i}),
                )
    for q, (_, c0, w) in enumerate(LANES):
        some = own_part[:, c0 : c0 + w] + base[:, c0 : c0 + w]
        drain(got[q], r3_r.at[q])
        for i in range(near):
            some = some + got[q][i].astype(f32)
        v_out[:, c0 : c0 + w] = some.astype(bf16)
        cols = pl.ds(c0, w)
        pltpu.make_async_copy(v_out.at[:, cols], out.at[:, cols], out_s).start()
    drain(conv.at[pl.ds(0, pairs)], mix_s)
    drain(seen_tab, tab_s)
    for n in range(near):
        drain(normed, ag_s.at[n])
    for q in range(lanes):
        drain(mid[q].at[:, :, pl.ds(0, pairs)], p3_s.at[q])
        drain(back[q].at[:, :, pl.ds(0, pairs)], r1_s.at[q])
        drain(slots[q].at[:, pl.ds(0, near)], r2_s.at[q])
        drain(part[q], r3_s.at[q])
    drain(v_out, out_s)


def body(
    out_gate, in_gate, conv_values, conv_taps, mix_gain, out_proj, residual, ffn_gain,
    routes, route_weights, shared_gate, shared_up, shared_down,
    expert_gate, expert_up, expert_down,
):
    length, channels = conv_values.shape
    row_count, width = residual.shape
    blocks = length // row_count
    unit = expert_gate.shape[2]
    shared_unit = shared_gate.shape[1]
    bf16, f32 = jnp.bfloat16, jnp.float32
    lanes = len(LANES)
    widths = [w for _, _, w in LANES]

    def per_lane(*shape):
        return [pltpu.VMEM(shape + (w,), bf16) for w in widths]

    def vmem(*shape, dtype=bf16):
        return pltpu.VMEM(shape, dtype)

    dma = pltpu.SemaphoreType.DMA
    near, pairs = RING - 1, len(PAIRS)
    plane = RING * RING * CORES * SLOTS
    mix_gain, ffn_gain = mix_gain.reshape(-1, 128), ffn_gain.reshape(1, width)
    routes, route_weights = routes.T, route_weights.T
    small = (conv_taps, mix_gain, ffn_gain, routes, route_weights)
    scratch = (
        [vmem(row_count, width)]
        + [vmem(*a.shape, dtype=a.dtype) for a in small]
        + [vmem(channels, length)] * 3
        + [vmem(RING, CORES * channels, width), vmem(row_count, width)]
        + [vmem(width, shared_unit), vmem(width, shared_unit), vmem(shared_unit, width)]
        + [vmem(width, unit), vmem(width, unit), vmem(unit, width)]
        + [vmem(channels, row_count + length, dtype=f32), vmem(8, 2 * row_count, dtype=f32)]
        + [vmem(8, 2 * row_count, dtype=f32)]
        + [vmem(blocks, channels, row_count)] * 2
        + [vmem(row_count, width, dtype=f32), vmem(row_count, width)]
        + [vmem(COLORS, RING, 8, plane, dtype=f32), vmem(near, COLORS, 8, plane, dtype=f32)]
        + [vmem(RING, RING, RING, CORES, SLOTS, width)] * 2
        + [vmem(RING, plane, unit, dtype=f32)] * 2
        + [vmem(RING, plane, unit), vmem(row_count, width, dtype=f32)]
        + per_lane(near, row_count)
        + per_lane(RING, RING, RING * CORES, SLOTS)
        + per_lane(RING, RING, RING * CORES, SLOTS)
        + per_lane(RING, RING, RING * CORES, SLOTS)
        + per_lane(near, row_count)
        + per_lane(near, row_count)
        + [dma((16,)), dma, dma, dma, dma((RING,)), dma, dma((near,)), dma((near,))]
        + [dma((lanes, near))]
        + [dma((lanes,))] * 10
        + [dma]
    )
    hbm = pl.BlockSpec(memory_space=pl.ANY)
    return pl.pallas_call(
        layer_kernel,
        out_shape=jax.ShapeDtypeStruct((row_count, width), bf16),
        in_specs=[hbm] * 16,
        out_specs=hbm,
        scratch_shapes=scratch,
        compiler_params=pltpu.CompilerParams(
            collective_id=0, has_side_effects=True, vmem_limit_bytes=67043328
        ),
        name="whole_layer",
    )(
        out_gate.T, in_gate.T, conv_values.T, conv_taps, mix_gain,
        out_proj.reshape(RING, CORES * channels, width), residual, ffn_gain,
        routes, route_weights, shared_gate, shared_up, shared_down,
        expert_gate[0], expert_up[0], expert_down[0],
    )


def solution(mesh):
    in_specs = (
        P("sp", "tp"),
        P("sp", "tp"),
        P("sp", "tp"),
        P(None, "tp"),
        P(),
        P(),
        P(("sp", "tp"), None),
        P(),
        P(("sp", "tp"), None),
        P(("sp", "tp"), None),
        P(),
        P(),
        P(),
        P(("sp", "tp"), None, None),
        P(("sp", "tp"), None, None),
        P(("sp", "tp"), None, None),
    )
    out_specs = P(("sp", "tp"), None)
    return jax.shard_map(body, mesh=mesh, in_specs=in_specs, out_specs=out_specs, check_vma=False)
```

time: 115 us -> 105 us (0.913)
  Pallas kernels: 113 us -> 103 us
    pallas_call x1, Pallas kernels: 113 us -> 103 us  [body(): pl.pallas_call(layer_kernel, out_shape=jax.ShapeDtypeStruct((row_count, w...]
where the time goes in v4:
time: 105 us
  Pallas kernels  103 us (98%)
  local copies, waits for them, and re-layouts  1.88 us (2%)
    pallas_call x1, Pallas kernels, body(): pl.pallas_call(layer_kernel, out_shape=jax.ShapeDtypeStruct((row_count, w...  103 us

profile of v4, /device:TPU:1, one launch (start us, length us, event | category | flops | bytes accessed | tf_op | source)
XLA Modules:
  0.0 104.5 jit_solution(4762472225422885301)
XLA Ops:
  0.0 102.6 %whole_layer.1 = bf16[128,2048]{1,0:T(8,128)(2,1)} custom-call(bf16[192,1024]{1,0:T(8,128)(2,1)} %bitcast.15, bf16[192,1024]{1,0:T(8,128)(2,1)} %bitcast.16, bf16[192,1024]{1,0:T(8,128)(2,1)} %bitcast.17, f32[3,192]{1,0:T(4,128)} %h_taps.1, f32[12,128]{1,0:T(8,128)} %bitcast.18, bf16[4,384,2048]{2,1,0:T(8,128)(2,1)} %bitcast.11, ...), custom_call_target="tpu_custom_call" | custom-call | tf_op jit(solution)/shard_map/whole_layer/pallas_call | solution.py:459
  102.6 1.9 %copy.18 = bf16[128,2048]{1,0:T(8,128)(2,1)} copy(bf16[128,2048]{1,0:T(8,128)(2,1)} %whole_layer.1) | data formatting | bytes 1048576

commit v5 on v4

--- a/solution.py
+++ b/solution.py
@@ -7,7 +7,7 @@
 
 AXES = ("z", "x", "y")
 ORDERS = (("z", "x", "y"), ("x", "y", "z"), ("y", "z", "x"))
-CHUNKS = ((256, 256, 256), (256, 256, 256), (128, 128, 256))
+CHUNKS = ((128, 128, 256), (256, 256, 128), (128, 128, 256), (128, 128, 128))
 RING = 4
 CORES = 2
 SLOTS = 8
@@ -276,7 +276,7 @@
         for d in FAR_FIRST:
             send(
                 pick[q].at[(at[second] + d) % RING, i], mid[q].at[lead(color, i, d)],
-                p2_s.at[q], p2_r.at[q], device(**{second: d}),
+                p2_s, p2_r.at[q], device(**{second: d}),
             )
         mid[q][lead(color, i, 0)] = pick[q][at[second], i]
 
@@ -300,15 +300,21 @@
             pick_rows(q, turn[q % 2])
 
     near, pairs = RING - 1, len(PAIRS)
+    eighth = arrived.shape[-1] // (RING * CORES)
+
+    def share(quarters=0, eighths=0):
+        return arrived.at[:, :, :, :, :, pl.ds(0, (quarters * CORES + eighths) * eighth)]
+
     for q, (color, c0, w) in enumerate(LANES):
         third = ORDERS[color][2]
         drain(mid[q].at[pl.ds(0, near)], p2_r.at[q])
-        drain(pick[q].at[pl.ds(0, near)], p2_s.at[q])
+        if q == lanes - COLORS:
+            drain(share(near), p2_s)
         for g, h in PAIRS:
             k = (at[third] + g) % RING * CORES + (core + h) % CORES
             send(
                 mid[q].at[:, :, k], piece(arrived, q, g, h),
-                p3_s.at[q], p3_r.at[q], device(h, **{third: g}),
+                p3_s, p3_r.at[q], device(h, **{third: g}),
             )
         piece(arrived, q, 0, 0)[...] = mid[q][:, :, at[third] * CORES + core]
 
@@ -350,7 +356,7 @@
             for g, h in PAIRS:
                 send(
                     piece(result, q, g, h), back[q].at[:, :, at[third] * CORES + core],
-                    r1_s.at[q], r1_r.at[q], device(-h, **{third: -g}),
+                    r1_s, r1_r.at[q], device(-h, **{third: -g}),
                 )
 
     for q, (color, c0, w) in enumerate(LANES):
@@ -360,7 +366,7 @@
         for d in FAR_FIRST:
             src = back[q].at[d] if color == 2 else back[q].at[:, d]
             send(
-                src, slots[q].at[:, at[second]], r2_s.at[q], r2_r.at[q], device(**{second: -d})
+                src, slots[q].at[:, at[second]], r2_s, r2_r.at[q], device(**{second: -d})
             )
         slots[q][:, at[second]] = back[q][0] if color == 2 else back[q][:, 0]
     for q, (color, c0, w) in enumerate(LANES):
@@ -380,7 +386,7 @@
             else:
                 part[q][i - 1] = some.astype(bf16)
                 send(
-                    part[q].at[i - 1], got[q].at[i - 1], r3_s.at[q], r3_r.at[q],
+                    part[q].at[i - 1], got[q].at[i - 1], r3_s, r3_r.at[q],
                     device(**{first: -i}),
                 )
     for q, (_, c0, w) in enumerate(LANES):
@@ -395,11 +401,10 @@
     drain(seen_tab, tab_s)
     for n in range(near):
         drain(normed, ag_s.at[n])
-    for q in range(lanes):
-        drain(mid[q].at[:, :, pl.ds(0, pairs)], p3_s.at[q])
-        drain(back[q].at[:, :, pl.ds(0, pairs)], r1_s.at[q])
-        drain(slots[q].at[:, pl.ds(0, near)], r2_s.at[q])
-        drain(part[q], r3_s.at[q])
+    drain(share(eighths=pairs), p3_s)
+    drain(share(eighths=pairs), r1_s)
+    drain(share(near), r2_s)
+    drain(arrived.at[pl.ds(0, near), pl.ds(0, 2)], r3_s)
     drain(v_out, out_s)
 
 
@@ -452,7 +457,7 @@
         + per_lane(near, row_count)
         + [dma((16,)), dma, dma, dma, dma((RING,)), dma, dma((near,)), dma((near,))]
         + [dma((lanes, near))]
-        + [dma((lanes,))] * 10
+        + [dma, dma((lanes,))] * 5
         + [dma]
     )
     hbm = pl.BlockSpec(memory_space=pl.ANY)

time: 105 us -> 103 us (0.981)
  Pallas kernels: 103 us -> 101 us
    pallas_call x1, Pallas kernels: 103 us -> 101 us  [body(): pl.pallas_call(layer_kernel, out_shape=jax.ShapeDtypeStruct((row_count, w...]
where the time goes in v5:
time: 103 us
  Pallas kernels  101 us (98%)
  local copies, waits for them, and re-layouts  1.88 us (2%)
    pallas_call x1, Pallas kernels, body(): pl.pallas_call(layer_kernel, out_shape=jax.ShapeDtypeStruct((row_count, w...  101 us

profile of v5, /device:TPU:1, one launch (start us, length us, event | category | flops | bytes accessed | tf_op | source)
XLA Modules:
  0.0 103.2 jit_solution(13362685899004437991)
XLA Ops:
  0.0 101.3 %whole_layer.1 = bf16[128,2048]{1,0:T(8,128)(2,1)} custom-call(bf16[192,1024]{1,0:T(8,128)(2,1)} %bitcast.15, bf16[192,1024]{1,0:T(8,128)(2,1)} %bitcast.16, bf16[192,1024]{1,0:T(8,128)(2,1)} %bitcast.17, f32[3,192]{1,0:T(4,128)} %h_taps.1, f32[12,128]{1,0:T(8,128)} %bitcast.18, bf16[4,384,2048]{2,1,0:T(8,128)(2,1)} %bitcast.11, ...), custom_call_target="tpu_custom_call" | custom-call | tf_op jit(solution)/shard_map/whole_layer/pallas_call | solution.py:464
  101.3 1.9 %copy.18 = bf16[128,2048]{1,0:T(8,128)(2,1)} copy(bf16[128,2048]{1,0:T(8,128)(2,1)} %whole_layer.1) | data formatting | bytes 1048576
